TPU v7x, 512 devices: a whole 4x8x8 slice. The times are simulated.
512 devices in a mesh: tp: 64 (over z, y), dp: 8 (over x, core).
Axes of the slice: x: 4, y: 8, z: 8, core: 2. Of those that a mesh axis runs over, the one named last changes fastest.
Arguments:
- tokens: bfloat16 [256, 4096], P(None, 'dp'), may hold values from -20 to 20
- norm_gain: float32 [2, 4096], P(None, 'dp'), may hold values from 0.1 to 1.9
- receptance: bfloat16 [2, 4096, 4096], P(None, 'dp', 'tp'), may hold values from -0.09375 to 0.09375
- key_proj: bfloat16 [2, 4096, 4096], P(None, 'dp', 'tp'), may hold values from -0.09375 to 0.09375
- value_proj: bfloat16 [2, 4096, 4096], P(None, 'dp', 'tp'), may hold values from -0.09375 to 0.09375
- decay_proj: bfloat16 [2, 4096, 4096], P(None, 'dp', 'tp'), may hold values from -0.09375 to 0.09375
- rate_proj: bfloat16 [2, 4096, 4096], P(None, 'dp', 'tp'), may hold values from -0.09375 to 0.09375
- gate_proj: bfloat16 [2, 4096, 4096], P(None, 'dp', 'tp'), may hold values from -0.09375 to 0.09375
- decay_base: float32 [2, 4096], P(None, 'tp'), may hold values from -6 to 1
- group_gain: float32 [2, 4096], P(None, 'tp'), may hold values from 0.1 to 1.9
- output_proj: bfloat16 [2, 4096, 4096], P(None, 'tp', 'dp'), may hold values from -0.09375 to 0.09375
- state: float32 [2, 256, 64, 4096], P(None, 'dp', 'tp'), may hold values from -3 to 3
Outputs:
- next_tokens: bfloat16 [256, 4096], P(None, 'dp')
- new_state: float32 [2, 256, 64, 4096], P(None, 'dp', 'tp')
All inputs are finite; a program needn't handle non-finite values.
Results may differ from a plain program's by a relative error of at most 0.0066.
Values may be sent and summed in bfloat16 or wider, within the bound.
A program may use at most 64 MiB of HBM per device.

v0:
```python
import jax
import jax.numpy as jnp
from jax import lax
from jax.sharding import PartitionSpec as P

D = 4096
HEAD = 64
LAYERS = 2


norm_floor = 0.1
group_floor = 0.5


def cut_along(x, dim, peers):
    shape = x.shape
    blocks = x.reshape(*shape[:dim], peers, shape[dim] // peers, *shape[dim + 1 :])
    return jnp.moveaxis(blocks, dim, 0)


def sent_and_summed(x, axis, dim):
    peers = lax.axis_size(axis)
    blocks = lax.all_to_all(cut_along(x, dim, peers), axis, 0, 0, tiled=True)
    return jnp.sum(blocks, axis=0)


def side_by_side(arrays, axis, dim, along):
    columns = [a.reshape(*a.shape[:along], -1) for a in arrays]
    both = jnp.concatenate(columns, axis=along)
    filled, at, outs = (sent_and_summed(both, axis, dim), 0, [])
    for a, column in zip(arrays, columns):
        section = filled[..., at : at + column.shape[along]]
        outs.append(section.reshape(*section.shape[:along], *a.shape[along:]))
        at += column.shape[along]
    return tuple(outs)


def laid_out(blocks, dim):
    shape = list(blocks.shape[1:])
    shape[dim] *= blocks.shape[0]
    return jnp.moveaxis(blocks, 0, dim).reshape(shape)


def copy_for_each(x, axis):
    peers = lax.axis_size(axis)
    return lax.all_to_all(jnp.broadcast_to(x[None], (peers, *x.shape)), axis, 0, 0, tiled=True)


def gathered_copies(x, axis, dim):
    return laid_out(copy_for_each(x, axis), dim)


def recurrence(state_block, recept_heads, key_heads, value_heads, decay_heads, rate_heads):
    log_rate = -jax.nn.softplus(-decay_heads) - 0.5
    forget = jnp.exp(-jnp.exp(log_rate))
    learn_rate = jax.nn.sigmoid(rate_heads)
    unit_key = key_heads * lax.rsqrt(jnp.sum(key_heads * key_heads, axis=-1, keepdims=True) + 1.0)
    scaled = key_heads * learn_rate
    removed = jnp.einsum("bhvk,bhk->bhv", state_block, -unit_key, precision=lax.Precision.HIGHEST)
    updated = (
        state_block * forget[:, :, None, :]
        + removed[..., None] * (unit_key * learn_rate)[:, :, None, :]
        + value_heads[..., None] * scaled[:, :, None, :]
    )
    read_out = jnp.einsum("bhvk,bhk->bhv", updated, recept_heads, precision=lax.Precision.HIGHEST)
    centre = read_out - jnp.mean(read_out, axis=-1, keepdims=True)
    normal = centre * lax.rsqrt(jnp.mean(centre * centre, axis=-1, keepdims=True) + group_floor)
    return (updated, normal)


def shards(
    tokens,
    norm_gain,
    receptance,
    key_proj,
    value_proj,
    decay_proj,
    rate_proj,
    gate_proj,
    decay_base,
    group_gain,
    output_proj,
    state,
):
    local_rows = state.shape[1]
    local_heads = state.shape[2]
    current = tokens
    finals = []
    for section_index in range(LAYERS):
        floats = current.astype(jnp.float32)
        squares = jnp.sum(floats * floats, axis=1)
        normed = (floats * norm_gain[section_index]).astype(jnp.bfloat16)
        part_recept = jnp.dot(normed, receptance[section_index], preferred_element_type=jnp.float32)
        part_key = jnp.dot(normed, key_proj[section_index], preferred_element_type=jnp.float32)
        part_value = jnp.dot(normed, value_proj[section_index], preferred_element_type=jnp.float32)
        part_decay = jnp.dot(normed, decay_proj[section_index], preferred_element_type=jnp.float32)
        part_rate = jnp.dot(normed, rate_proj[section_index], preferred_element_type=jnp.float32)
        part_gate = jnp.dot(normed, gate_proj[section_index], preferred_element_type=jnp.float32)
        summed = side_by_side(
            (part_recept, part_key, part_value, part_decay, part_rate, part_gate, squares),
            "dp",
            0,
            1,
        )
        own_squares = summed[6]
        inv_rms = lax.rsqrt(own_squares / D + norm_floor)

        def by_head(term):
            rounded = lax.optimization_barrier((inv_rms[:, None] * term).astype(jnp.bfloat16))
            return rounded.astype(jnp.float32).reshape(local_rows, local_heads, HEAD)

        decay_heads = by_head(summed[3]) + decay_base[section_index].reshape(1, local_heads, HEAD)
        updated, normal = recurrence(
            state[section_index].reshape(local_rows, local_heads, HEAD, HEAD),
            by_head(summed[0]),
            by_head(summed[1]),
            by_head(summed[2]),
            decay_heads,
            by_head(summed[4]),
        )
        finals.append(updated.reshape(local_rows, local_heads, HEAD * HEAD))
        gate_value = jax.nn.sigmoid(by_head(summed[5]).reshape(local_rows, local_heads * HEAD))
        mixed_heads = (
            normal.reshape(local_rows, local_heads * HEAD) * group_gain[section_index] * gate_value
        ).astype(jnp.bfloat16)
        weights_out = output_proj[section_index]

        def apply_out(piece, begin, weights_out=weights_out):
            return jnp.dot(piece, weights_out, preferred_element_type=jnp.float32)

        partial_out = apply_out(gathered_copies(mixed_heads, "dp", 0), jnp.int32(0))
        width = floats.shape[1] // lax.axis_size("tp")
        offset = lax.axis_index("tp") * width
        share = sent_and_summed(partial_out, "tp", 1)
        mine = lax.dynamic_slice_in_dim(floats, offset, width, 1)
        new_share = (mine + share).astype(jnp.bfloat16)
        current = gathered_copies(new_share, "tp", 1)
    return (current, jnp.stack(finals))


def solution(mesh):
    return jax.shard_map(
        shards,
        mesh=mesh,
        in_specs=(
            P(None, "dp"),
            P(None, "dp"),
            P(None, "dp", "tp"),
            P(None, "dp", "tp"),
            P(None, "dp", "tp"),
            P(None, "dp", "tp"),
            P(None, "dp", "tp"),
            P(None, "dp", "tp"),
            P(None, "tp"),
            P(None, "tp"),
            P(None, "tp", "dp"),
            P(None, "dp", "tp", None),
        ),
        out_specs=(P(None, "dp"), P(None, "dp", "tp", None)),
        check_vma=False,
    )
```

profile of v0, /device:TPU:1, one launch (start us, length us, event | category | flops | bytes accessed | tf_op | source)
XLA Modules:
  0.0 177.7 jit_solution(9545920137417492154)
XLA Ops:
  8.7 10.2 %all-to-all-start = ((f32[8,32,385]{2,1,0:T(8,128)}), f32[8,32,385]{2,1,0:T(8,128)S(1)}, u32[]{:S(2)}, u32[]{:S(2)}) async-start(f32[8,32,385]{2,1,0:T(8,128)} %concatenate.13), calls=%async_computation | async-start | bytes 1048576 | tf_op jit(solution)/shard_map/all_to_all | solution.py:23
  19.0 3.5 %slice_reduce_fusion = (f32[32,4096]{1,0:T(8,128)S(1)}, f32[32,4096]{1,0:T(8,128)}) fusion(f32[2,32,1,4096]{3,2,1,0:T(1,128)S(1)} %copy-done), kind=kLoop, calls=%fused_computation.26 | loop fusion | bytes 2097152 | tf_op jit(solution)/shard_map/slice | solution.py:114
  22.4 1.5 reshape_squeeze.8
  24.6 3.7 %all-to-all-done = f32[8,32,385]{2,1,0:T(8,128)S(1)} async-done(((f32[8,32,385]{2,1,0:T(8,128)}), f32[8,32,385]{2,1,0:T(8,128)S(1)}, u32[]{:S(2)}, u32[]{:S(2)}) %all-to-all-start) | async-done | bytes 394272 | tf_op jit(solution)/shard_map/all_to_all | solution.py:23
  28.9 1.7 fusion.88
  30.6 1.5 fusion.4
  33.2 4.2 %all-to-all-start.1 = ((bf16[8,2,1024]{2,1,0:T(2,128)(2,1)}), bf16[8,2,1024]{2,1,0:T(2,128)(2,1)S(1)}, u32[]{:S(2)}, u32[]{:S(2)}) async-start(bf16[8,2,1024]{2,1,0:T(2,128)(2,1)} %reshape.441), calls=%async_computation.1 | async-start | bytes 65536 | tf_op jit(solution)/shard_map/all_to_all | solution.py:46
  37.6 4.6 %all-to-all-done.1 = bf16[8,2,1024]{2,1,0:T(2,128)(2,1)S(1)} async-done(((bf16[8,2,1024]{2,1,0:T(2,128)(2,1)}), bf16[8,2,1024]{2,1,0:T(2,128)(2,1)S(1)}, u32[]{:S(2)}, u32[]{:S(2)}) %all-to-all-start.1) | async-done | bytes 32800 | tf_op jit(solution)/shard_map/all_to_all | solution.py:46
  42.5 1.1 copy.79
  43.6 11.8 %all-to-all-start.2 = ((f32[64,256,8]{1,2,0:T(8,128)}), f32[64,256,8]{1,2,0:T(8,128)S(1)}, u32[]{:S(2)}, u32[]{:S(2)}) async-start(f32[64,256,8]{1,2,0:T(8,128)} %copy.79), calls=%async_computation.2 | async-start | bytes 1048576 | tf_op jit(solution)/shard_map/all_to_all | solution.py:23
  55.5 17.3 %all-to-all-done.2 = f32[64,256,8]{1,2,0:T(8,128)S(1)} async-done(((f32[64,256,8]{1,2,0:T(8,128)}), f32[64,256,8]{1,2,0:T(8,128)S(1)}, u32[]{:S(2)}, u32[]{:S(2)}) %all-to-all-start.2) | async-done | bytes 524320 | tf_op jit(solution)/shard_map/all_to_all | solution.py:23
  73.7 6.5 %all-to-all-start.3 = ((bf16[64,256,8]{1,2,0:T(8,128)(2,1)}), bf16[64,256,8]{1,2,0:T(8,128)(2,1)S(1)}, u32[]{:S(2)}, u32[]{:S(2)}) async-start(bf16[64,256,8]{1,2,0:T(8,128)(2,1)} %broadcast_in_dim.9), calls=%async_computation.3 | async-start | bytes 524288 | tf_op jit(solution)/shard_map/all_to_all | solution.py:46
  80.3 12.4 %all-to-all-done.3 = bf16[64,256,8]{1,2,0:T(8,128)(2,1)S(1)} async-done(((bf16[64,256,8]{1,2,0:T(8,128)(2,1)}), bf16[64,256,8]{1,2,0:T(8,128)(2,1)S(1)}, u32[]{:S(2)}, u32[]{:S(2)}) %all-to-all-start.3) | async-done | bytes 262176 | tf_op jit(solution)/shard_map/all_to_all | solution.py:46
  100.7 6.9 %all-to-all-start.4 = ((f32[8,32,385]{2,1,0:T(8,128)}), f32[8,32,385]{2,1,0:T(8,128)S(1)}, u32[]{:S(2)}, u32[]{:S(2)}) async-start(f32[8,32,385]{2,1,0:T(8,128)} %concatenate.15), calls=%async_computation.4 | async-start | bytes 1048576 | tf_op jit(solution)/shard_map/all_to_all | solution.py:23
  108.0 9.0 %all-to-all-done.4 = f32[8,32,385]{2,1,0:T(8,128)S(1)} async-done(((f32[8,32,385]{2,1,0:T(8,128)}), f32[8,32,385]{2,1,0:T(8,128)S(1)}, u32[]{:S(2)}, u32[]{:S(2)}) %all-to-all-start.4) | async-done | bytes 394272 | tf_op jit(solution)/shard_map/all_to_all | solution.py:23
  117.4 1.7 fusion.89
  119.2 1.5 fusion
  121.8 4.2 %all-to-all-start.5 = ((bf16[8,2,1024]{2,1,0:T(2,128)(2,1)}), bf16[8,2,1024]{2,1,0:T(2,128)(2,1)S(1)}, u32[]{:S(2)}, u32[]{:S(2)}) async-start(bf16[8,2,1024]{2,1,0:T(2,128)(2,1)} %reshape.443), calls=%async_computation.5 | async-start | bytes 65536 | tf_op jit(solution)/shard_map/all_to_all | solution.py:46
  126.1 4.6 %all-to-all-done.5 = bf16[8,2,1024]{2,1,0:T(2,128)(2,1)S(1)} async-done(((bf16[8,2,1024]{2,1,0:T(2,128)(2,1)}), bf16[8,2,1024]{2,1,0:T(2,128)(2,1)S(1)}, u32[]{:S(2)}, u32[]{:S(2)}) %all-to-all-start.5) | async-done | bytes 32800 | tf_op jit(solution)/shard_map/all_to_all | solution.py:46
  132.2 5.5 %all-to-all-start.6 = ((f32[64,256,8]{1,2,0:T(8,128)}), f32[64,256,8]{1,2,0:T(8,128)}, u32[]{:S(2)}, u32[]{:S(2)}) async-start(f32[64,256,8]{1,2,0:T(8,128)} %copy.91), calls=%async_computation.6 | async-start | bytes 1048576 | tf_op jit(solution)/shard_map/all_to_all | solution.py:23
  138.3 1.4 mul.417
  139.8 1.4 mul.416
  141.3 1.5 mul.414
  144.2 1.4 mul.421
  145.6 1.5 mul.420
  147.2 1.4 mul.418
  148.6 6.4 %all-to-all-done.6 = f32[64,256,8]{1,2,0:T(8,128)} async-done(((f32[64,256,8]{1,2,0:T(8,128)}), f32[64,256,8]{1,2,0:T(8,128)}, u32[]{:S(2)}, u32[]{:S(2)}) %all-to-all-start.6) | async-done | bytes 524320 | tf_op jit(solution)/shard_map/all_to_all | solution.py:23
  155.1 1.2 reduce_sum.119
  157.7 6.9 %all-to-all-start.7 = ((bf16[64,256,8]{1,2,0:T(8,128)(2,1)}), bf16[64,256,8]{1,2,0:T(8,128)(2,1)S(1)}, u32[]{:S(2)}, u32[]{:S(2)}) async-start(bf16[64,256,8]{1,2,0:T(8,128)(2,1)} %broadcast_in_dim.11), calls=%async_computation.7 | async-start | bytes 524288 | tf_op jit(solution)/shard_map/all_to_all | solution.py:46
  164.7 4.2 %add_add_fusion.1 = (f32[1,32,1,4096]{3,2,1,0:T(1,128)S(1)}, f32[1,32,1,4096]{3,2,1,0:T(1,128)S(1)}) fusion(f32[1,32,1,4096]{3,2,1,0:T(1,128)S(1)} %copy-done.3, f32[1,32,1,4096]{3,2,1,0:T(1,128)S(1)} %copy-done.4, f32[1,32,1,4096]{3,2,1,0:T(1,128)S(1)} %copy-done.5, f32[2,32,1,4096]{3,2,1,0:T(1,128)S(1)} %copy-done, f32[1,32,1,4096]{3,2,1,0:T(1,128)S(1)} %copy-done.6, ...), kind=kLoop, calls=%fused_computation.17 | loop fusion | flops 786432 | bytes 5242880 | tf_op jit(solution)/shard_map/add | solution.py:61
  168.9 2.1 %pad_maximum_fusion = f32[2,32,1,4096]{3,2,1,0:T(1,128)} fusion(f32[1,32,1,4096]{3,2,1,0:T(1,128)S(1)} %get-tuple-element.11, f32[1,32,1,4096]{3,2,1,0:T(1,128)S(1)} %get-tuple-element.10), kind=kLoop, calls=%fused_computation.2 | loop fusion | flops 262144 | bytes 2097152 | tf_op jit(solution)/shard_map/stack | solution.py:138
  171.0 5.9 %all-to-all-done.7 = bf16[64,256,8]{1,2,0:T(8,128)(2,1)S(1)} async-done(((bf16[64,256,8]{1,2,0:T(8,128)(2,1)}), bf16[64,256,8]{1,2,0:T(8,128)(2,1)S(1)}, u32[]{:S(2)}, u32[]{:S(2)}) %all-to-all-start.7) | async-done | bytes 262176 | tf_op jit(solution)/shard_map/all_to_all | solution.py:46
  (123 shorter events, 27.7 us)
Async XLA Ops:
  0.6 1.1 copy-start.20
  1.9 0.9 copy-start.7
  2.8 0.9 copy-start.9
  3.7 0.9 copy-start.11
  4.6 0.9 copy-start.13
  5.5 0.9 copy-start.15
  6.4 0.9 copy-start.17
  7.8 11.2 %copy-start = (f32[2,32,1,4096]{3,2,1,0:T(1,128)S(1)}, f32[2,32,1,4096]{3,2,1,0:T(1,128)}, u32[]{:S(2)}) copy-start(f32[2,32,1,4096]{3,2,1,0:T(1,128)} %param.23) | copy-start | bytes 3145732
  8.7 19.6 %all-to-all-start = ((f32[8,32,385]{2,1,0:T(8,128)}), f32[8,32,385]{2,1,0:T(8,128)S(1)}, u32[]{:S(2)}, u32[]{:S(2)}) async-start(f32[8,32,385]{2,1,0:T(8,128)} %concatenate.13), calls=%async_computation | async-start | bytes 1048576 | tf_op jit(solution)/shard_map/all_to_all | solution.py:23
  22.4 1.5 copy-start.21
  23.9 0.7 copy-start.22
  32.4 5.0 %copy-start.19 = (bf16[2,64,512]{2,1,0:T(8,128)(2,1)S(1)}, bf16[2,64,512]{2,1,0:T(8,128)(2,1)}, u32[]{:S(2)}) copy-start(bf16[2,64,512]{2,1,0:T(8,128)(2,1)} %param.22) | copy-start | bytes 393220
  33.2 8.9 %all-to-all-start.1 = ((bf16[8,2,1024]{2,1,0:T(2,128)(2,1)}), bf16[8,2,1024]{2,1,0:T(2,128)(2,1)S(1)}, u32[]{:S(2)}, u32[]{:S(2)}) async-start(bf16[8,2,1024]{2,1,0:T(2,128)(2,1)} %reshape.441), calls=%async_computation.1 | async-start | bytes 65536 | tf_op jit(solution)/shard_map/all_to_all | solution.py:46
  43.6 29.2 %all-to-all-start.2 = ((f32[64,256,8]{1,2,0:T(8,128)}), f32[64,256,8]{1,2,0:T(8,128)S(1)}, u32[]{:S(2)}, u32[]{:S(2)}) async-start(f32[64,256,8]{1,2,0:T(8,128)} %copy.79), calls=%async_computation.2 | async-start | bytes 1048576 | tf_op jit(solution)/shard_map/all_to_all | solution.py:23
  73.7 19.0 %all-to-all-start.3 = ((bf16[64,256,8]{1,2,0:T(8,128)(2,1)}), bf16[64,256,8]{1,2,0:T(8,128)(2,1)S(1)}, u32[]{:S(2)}, u32[]{:S(2)}) async-start(bf16[64,256,8]{1,2,0:T(8,128)(2,1)} %broadcast_in_dim.9), calls=%async_computation.3 | async-start | bytes 524288 | tf_op jit(solution)/shard_map/all_to_all | solution.py:46
  92.7 0.7 copy-start.1
  93.8 0.9 copy-start.8
  94.7 0.9 copy-start.10
  95.7 0.9 copy-start.12
  96.6 0.9 copy-start.14
  97.5 0.9 copy-start.16
  98.4 0.9 copy-start.18
  100.7 16.3 %all-to-all-start.4 = ((f32[8,32,385]{2,1,0:T(8,128)}), f32[8,32,385]{2,1,0:T(8,128)S(1)}, u32[]{:S(2)}, u32[]{:S(2)}) async-start(f32[8,32,385]{2,1,0:T(8,128)} %concatenate.15), calls=%async_computation.4 | async-start | bytes 1048576 | tf_op jit(solution)/shard_map/all_to_all | solution.py:23
  121.8 8.9 %all-to-all-start.5 = ((bf16[8,2,1024]{2,1,0:T(2,128)(2,1)}), bf16[8,2,1024]{2,1,0:T(2,128)(2,1)S(1)}, u32[]{:S(2)}, u32[]{:S(2)}) async-start(bf16[8,2,1024]{2,1,0:T(2,128)(2,1)} %reshape.443), calls=%async_computation.5 | async-start | bytes 65536 | tf_op jit(solution)/shard_map/all_to_all | solution.py:46
  132.2 22.9 %all-to-all-start.6 = ((f32[64,256,8]{1,2,0:T(8,128)}), f32[64,256,8]{1,2,0:T(8,128)}, u32[]{:S(2)}, u32[]{:S(2)}) async-start(f32[64,256,8]{1,2,0:T(8,128)} %copy.91), calls=%async_computation.6 | async-start | bytes 1048576 | tf_op jit(solution)/shard_map/all_to_all | solution.py:23
  141.3 1.5 copy-start.2
  147.2 17.5 %copy-start.5 = (f32[1,32,1,4096]{3,2,1,0:T(1,128)S(1)}, f32[1,32,1,4096]{3,2,1,0:T(1,128)}, u32[]{:S(2)}) copy-start(f32[1,32,1,4096]{3,2,1,0:T(1,128)} %mul.414) | copy-start | bytes 1572868
  147.2 17.5 %copy-start.6 = (f32[1,32,1,4096]{3,2,1,0:T(1,128)S(1)}, f32[1,32,1,4096]{3,2,1,0:T(1,128)}, u32[]{:S(2)}) copy-start(f32[1,32,1,4096]{3,2,1,0:T(1,128)} %mul.421) | copy-start | bytes 1572868
  155.1 9.6 %copy-start.4 = (f32[1,32,1,4096]{3,2,1,0:T(1,128)S(1)}, f32[1,32,1,4096]{3,2,1,0:T(1,128)}, u32[]{:S(2)}) copy-start(f32[1,32,1,4096]{3,2,1,0:T(1,128)} %mul.416) | copy-start | bytes 1572868
  156.2 8.4 %copy-start.3 = (f32[1,32,1,4096]{3,2,1,0:T(1,128)S(1)}, f32[1,32,1,4096]{3,2,1,0:T(1,128)}, u32[]{:S(2)}) copy-start(f32[1,32,1,4096]{3,2,1,0:T(1,128)} %mul.417) | copy-start | bytes 1572868
  157.7 19.2 %all-to-all-start.7 = ((bf16[64,256,8]{1,2,0:T(8,128)(2,1)}), bf16[64,256,8]{1,2,0:T(8,128)(2,1)S(1)}, u32[]{:S(2)}, u32[]{:S(2)}) async-start(bf16[64,256,8]{1,2,0:T(8,128)(2,1)} %broadcast_in_dim.11), calls=%async_computation.7 | async-start | bytes 524288 | tf_op jit(solution)/shard_map/all_to_all | solution.py:46
where the time goes:
time: 180 us; the launch traced here: 178 us
  waiting for transfers between devices  64 us (36%)
  starting transfers between devices  56.3 us (31%)
  local copies, waits for them, and re-layouts  34.6 us (19%)
  other arithmetic  12.4 us (7%)
  matrix products  9.27 us (5%)
    all_to_all x4, waiting for transfers between devices, sent_and_summed(): blocks = lax.all_to_all(cut_along(x, dim, peers), axis, 0, 0, tiled=True)  36.5 us
    all_to_all x4, starting transfers between devices, sent_and_summed(): blocks = lax.all_to_all(cut_along(x, dim, peers), axis, 0, 0, tiled=True)  34.4 us
    all_to_all x4, waiting for transfers between devices, copy_for_each(): lax.all_to_all(jnp.broadcast_to(x[None], (peers, *x.shape)), axis, 0, 0,...  27.5 us
    all_to_all x4, starting transfers between devices, copy_for_each(): lax.all_to_all(jnp.broadcast_to(x[None], (peers, *x.shape)), axis, 0, 0,...  21.8 us
    unnamed x54, local copies, waits for them, and re-layouts  13 us
    add x1, other arithmetic, recurrence(): state_block * forget[:, :, None, :]  4.23 us
  transfers between devices with their start and end apart: 8, of which 8 were waited for; matrix products, arithmetic and copies ran while one was open for 13% of the time, Pallas kernels for 0%

commit v1 on v0

v1 whole, which is shorter than its diff:
```python
import jax
import jax.numpy as jnp
from jax import lax
from jax.experimental import pallas as pl
from jax.experimental.pallas import tpu as pltpu
from jax.sharding import PartitionSpec as P

D = 4096
HEAD = 64
LAYERS = 2
ROWS = 32
WIDE = 512
LANES = 128

norm_floor = 0.1
group_floor = 0.5

MESH = pl.DeviceIdType.MESH
RING8 = (4, 3, 5, 2, 6, 1, 7)
TP_OFFSETS = sorted(
    ((a, b) for a in range(8) for b in range(8) if (a, b) != (0, 0)),
    key=lambda ab: -(min(ab[0], 8 - ab[0]) + min(ab[1], 8 - ab[1])),
)


def iota(shape, dim):
    return lax.broadcasted_iota(jnp.int32, shape, dim)


def two_terms(x):
    high = x.astype(jnp.bfloat16)
    low = (x - high.astype(jnp.float32)).astype(jnp.bfloat16)
    return jnp.concatenate([high, low], axis=1)


def dot(a, b):
    return jnp.dot(a, b, preferred_element_type=jnp.float32)


def wait_for(ref, sem):
    pltpu.make_async_copy(ref, ref, sem).wait()


def body(
    tokens_ref,
    gain_ref,
    w0,
    w1,
    w2,
    w3,
    w4,
    w5,
    decay_ref,
    group_ref,
    out_proj_ref,
    state_ref,
    next_ref,
    new_state_ref,
    tokens,
    weights,
    wout,
    wdiag,
    state,
    part_send,
    part_recv,
    sq_send,
    sq_recv,
    mixed_all,
    out_send,
    out_recv,
    share,
    x_all,
    vec_g,
    vec_f,
    vec_s,
    vec_u,
    vec_v,
    read_rows,
    load_sem,
    late_sem,
    part_ssem,
    part_rsem,
    sq_ssem,
    sq_rsem,
    mix_ssem,
    mix_rsem,
    out_ssem,
    out_rsem,
    x_ssem,
    x_rsem,
    row_sem,
):
    tp = lax.axis_index("tp")
    dp = lax.axis_index("dp")
    z = tp // 8
    y = lax.rem(tp, 8)
    dp_peers = [(tp, lax.rem(dp + o, 8)) for o in RING8]
    y_peers = [(z * 8 + lax.rem(y + o, 8), dp) for o in RING8]
    z_peers = [(lax.rem(z + o, 8) * 8 + y, dp) for o in RING8]
    tp_peers = [(lax.rem(z + a, 8) * 8 + lax.rem(y + b, 8), dp) for a, b in TP_OFFSETS]

    barrier = pltpu.get_barrier_semaphore()
    for peer in dp_peers + y_peers + z_peers:
        pl.semaphore_signal(barrier, inc=1, device_id=peer, device_id_type=MESH)

    loads = [[], []]
    first = pltpu.make_async_copy(tokens_ref, tokens, load_sem.at[0])
    first.start()
    loads[0].append(first)
    for b in range(LAYERS):
        for n, w in enumerate((w0, w1, w2, w3, w4, w5)):
            copy = pltpu.make_async_copy(
                w.at[b], weights.at[b, pl.ds(n * HEAD, HEAD)], (load_sem if b == 0 else late_sem).at[n + 1]
            )
            copy.start()
            loads[b].append(copy)
        if b == 0:
            state_copy = pltpu.make_async_copy(state_ref, state, late_sem.at[0])
            state_copy.start()
            wout_copy = pltpu.make_async_copy(out_proj_ref, wout, load_sem.at[7])
            wout_copy.start()

    lane = iota((ROWS, LANES), 1)
    row = iota((ROWS, LANES), 0)
    low_half = lane < HEAD
    eye = (lane == row).astype(jnp.float32)
    pick = (lane % HEAD) // 2 == row
    pick_own = lane % HEAD == 2 * row + lane // HEAD
    ones = jnp.full((2 * LANES, LANES), 1.0, jnp.bfloat16)
    k_of = iota((2 * LANES, LANES), 0)
    l_of = iota((2 * LANES, LANES), 1)
    by_parity = ((k_of // HEAD) % 2 == l_of % 2).astype(jnp.float32).astype(jnp.bfloat16)
    by_half = ((k_of // HEAD) % 2 == l_of // HEAD).astype(jnp.float32).astype(jnp.bfloat16)

    sends = []

    def project(b, columns):
        squares = columns[0] * columns[0]
        for c in columns[1:]:
            squares = squares + c * c
        totals = dot(two_terms(squares), ones)
        for o in range(8):
            sq_send[b, o] = jnp.sum(totals[o * ROWS : (o + 1) * ROWS] * eye, axis=0, keepdims=True)
        normed = jnp.concatenate(
            [(c * gain_ref[b : b + 1, n * LANES : (n + 1) * LANES]).astype(jnp.bfloat16) for n, c in enumerate(columns)],
            axis=1,
        )
        for copy in loads[b][-6:]:
            copy.wait()
        part = lax.dot_general(
            normed, weights[b], (((1,), (1,)), ((), ())), preferred_element_type=jnp.float32
        ).astype(jnp.bfloat16)
        for o in range(8):
            part_send[b, o] = part[o * ROWS : (o + 1) * ROWS]

    def send_parts(b):
        for i, peer in enumerate(dp_peers):
            for src, dst, ssem, rsem in (
                (part_send, part_recv, part_ssem, part_rsem),
                (sq_send, sq_recv, sq_ssem, sq_rsem),
            ):
                pltpu.make_async_remote_copy(
                    src_ref=src.at[b, peer[1]],
                    dst_ref=dst.at[b, i],
                    send_sem=ssem.at[b],
                    recv_sem=rsem.at[b],
                    device_id=peer,
                    device_id_type=MESH,
                ).start()
        sends.append((part_recv.at[b], part_ssem.at[b]))
        sends.append((sq_recv.at[b], sq_ssem.at[b]))

    def mix(b):
        wait_for(sq_recv.at[b], sq_rsem.at[b])
        square = sq_send[b, dp]
        for i in range(7):
            square = square + sq_recv[b, i]
        inv = lax.rsqrt(jnp.sum(square * eye, axis=1, keepdims=True) / D + norm_floor)
        wait_for(part_recv.at[b], part_rsem.at[b])
        total = part_send[b, dp].astype(jnp.float32)
        for i in range(7):
            total = total + part_recv[b, i].astype(jnp.float32)
        heads = (total * inv).astype(jnp.bfloat16).astype(jnp.float32)
        both = []
        for n in range(3):
            tile = heads[:, n * LANES : (n + 1) * LANES]
            turned = pltpu.roll(tile, HEAD, 1)
            both.append(jnp.where(low_half, tile, turned))
            both.append(jnp.where(low_half, turned, tile))
        recept, keys, values, decay_in, rate_in, gate_in = both
        base = decay_ref[b : b + 1, :]
        decay = jnp.concatenate([base, base], axis=1) + decay_in
        forget = jnp.exp(-jnp.exp(-jax.nn.softplus(-decay) - 0.5))
        learn = jax.nn.sigmoid(rate_in)
        norm = lax.rsqrt(0.5 * jnp.sum(keys * keys, axis=1, keepdims=True) + 1.0)
        scaled = keys * learn
        with_scaled = 0.5 * jnp.sum(scaled * recept, axis=1, keepdims=True)
        unit = keys * norm
        vec_g[...] = forget * recept - (with_scaled * norm) * unit
        vec_f[...] = forget
        vec_s[...] = scaled
        vec_u[...] = unit * norm
        vec_v[...] = values
        for c in range(4):
            terms = jnp.concatenate(
                [state[b, r] * vec_g[r : r + 1, :] for r in range(c * 8, c * 8 + 8)], axis=0
            )
            sums = dot(two_terms(terms), by_parity)
            for r in range(8):
                at = c * 8 + r
                chosen = jnp.where(pick, sums[r * ROWS : (r + 1) * ROWS], 0.0)
                read_rows[at : at + 1, :] = jnp.sum(chosen, axis=0, keepdims=True)
        read = read_rows[...] + values * with_scaled
        centre = read - jnp.mean(read, axis=1, keepdims=True)
        normal = centre * lax.rsqrt(jnp.mean(centre * centre, axis=1, keepdims=True) + group_floor)
        gain = group_ref[b : b + 1, :]
        mixed = (normal * jnp.concatenate([gain, gain], axis=1) * jax.nn.sigmoid(gate_in)).astype(jnp.bfloat16)
        mixed_all[b, dp] = jnp.where(low_half[:16], mixed[:16], mixed[16:])

    def send_mixed(b):
        for peer in dp_peers:
            pltpu.make_async_remote_copy(
                src_ref=mixed_all.at[b, dp],
                dst_ref=mixed_all.at[b, dp],
                send_sem=mix_ssem.at[b],
                recv_sem=mix_rsem.at[b],
                device_id=peer,
                device_id_type=MESH,
            ).start()
        sends.append((mixed_all.at[b, pl.ds(0, 7)], mix_ssem.at[b]))

    def project_out(b):
        wait_for(mixed_all.at[b, pl.ds(0, 7)], mix_rsem.at[b])
        rows = mixed_all[b].reshape(8 * 16, LANES)
        for half in range(2):
            term = dot(rows, wdiag[b, half]).astype(jnp.bfloat16)
            for o in range(8):
                for c in range(4):
                    out_send[b, (o * 2 + half) * 4 + c] = term[o * 16 : (o + 1) * 16, c * LANES : (c + 1) * LANES]

    def send_out(b):
        for i, peer in enumerate(tp_peers):
            pltpu.make_async_remote_copy(
                src_ref=out_send.at[b, peer[0]],
                dst_ref=out_recv.at[b, i],
                send_sem=out_ssem.at[b],
                recv_sem=out_rsem.at[b],
                device_id=peer,
                device_id_type=MESH,
            ).start()
        sends.append((out_recv.at[b], out_ssem.at[b]))

    def update_state(b):
        for c in range(4):
            terms = jnp.concatenate(
                [
                    jnp.where(pick_own, vec_v[r : r + 1, :], 0.0) - state[b, r] * vec_u[r : r + 1, :]
                    for r in range(c * 8, c * 8 + 8)
                ],
                axis=0,
            )
            sums = dot(two_terms(terms), by_half)
            for r in range(8):
                at = c * 8 + r
                new_state_ref[b, at] = (
                    state[b, at] * vec_f[at : at + 1, :]
                    + sums[r * ROWS : (r + 1) * ROWS] * vec_s[at : at + 1, :]
                )

    def finish_share(b, mine):
        wait_for(out_recv.at[b], out_rsem.at[b])
        parts = [out_send[b, tp].astype(jnp.float32)] + [jnp.zeros((16, LANES), jnp.float32)] * 3
        for i in range(63):
            parts[(i + 1) % 4] = parts[(i + 1) % 4] + out_recv[b, i].astype(jnp.float32)
        total = (parts[0] + parts[1]) + (parts[2] + parts[3])
        new = (mine.astype(jnp.float32) + total).astype(jnp.bfloat16)
        share[b] = new
        x_all[b, tp] = new

    def send_share(b):
        for peer in tp_peers:
            pltpu.make_async_remote_copy(
                src_ref=share.at[b],
                dst_ref=x_all.at[b, tp],
                send_sem=x_ssem.at[b],
                recv_sem=x_rsem.at[b],
                device_id=peer,
                device_id_type=MESH,
            ).start()
        sends.append((x_all.at[b, pl.ds(0, 63)], x_ssem.at[b]))

    first.wait()
    project(0, [tokens[:, c * LANES : (c + 1) * LANES].astype(jnp.float32) for c in range(4)])
    pl.semaphore_wait(barrier, 21)
    send_parts(0)
    for peer in z_peers:
        pl.semaphore_signal(row_sem, inc=1, device_id=peer, device_id_type=MESH)
    wout_copy.wait()
    wdiag[...] = jnp.zeros_like(wdiag)
    for b in range(LAYERS):
        wdiag[b, 0, 0:HEAD] = wout[b]
        wdiag[b, 1, HEAD : 2 * HEAD] = wout[b]
    state_copy.wait()
    mix(0)
    send_mixed(0)
    pl.semaphore_wait(row_sem, 7)
    project_out(0)
    send_out(0)
    update_state(0)
    at_row = pl.multiple_of((tp // 4) * 16, 16)
    at_column = pl.multiple_of(lax.rem(tp, 4) * LANES, LANES)
    finish_share(0, tokens[pl.ds(at_row, 16), pl.ds(at_column, LANES)])
    send_share(0)
    wait_for(x_all.at[0, pl.ds(0, 63)], x_rsem.at[0])

    columns = [
        jnp.concatenate([x_all[0, g * 4 + c].astype(jnp.float32) for g in range(16)], axis=0) for c in range(4)
    ]
    project(1, columns)
    send_parts(1)
    mix(1)
    send_mixed(1)
    project_out(1)
    send_out(1)
    update_state(1)
    finish_share(1, share[0])
    send_share(1)
    wait_for(x_all.at[1, pl.ds(0, 63)], x_rsem.at[1])
    for g in range(16):
        for c in range(4):
            next_ref[g * 16 : (g + 1) * 16, c * LANES : (c + 1) * LANES] = x_all[1, g * 4 + c]
    for ref, sem in sends:
        wait_for(ref, sem)


def shards(
    tokens,
    norm_gain,
    receptance,
    key_proj,
    value_proj,
    decay_proj,
    rate_proj,
    gate_proj,
    decay_base,
    group_gain,
    output_proj,
    state,
):
    flat = [jnp.swapaxes(w, 1, 2) for w in (receptance, key_proj, value_proj, decay_proj, rate_proj, gate_proj)]
    remote = pl.BlockSpec(memory_space=pltpu.HBM)
    local = pl.BlockSpec(memory_space=pltpu.VMEM)
    f32, bf16 = jnp.float32, jnp.bfloat16
    dma = pltpu.SemaphoreType.DMA
    current, updated = pl.pallas_call(
        body,
        out_shape=(
            jax.ShapeDtypeStruct((256, WIDE), bf16),
            jax.ShapeDtypeStruct((LAYERS, ROWS, 32, LANES), f32),
        ),
        in_specs=[remote, local] + [remote] * 6 + [local, local, remote, remote],
        out_specs=(local, local),
        scratch_shapes=[
            pltpu.VMEM((256, WIDE), bf16),
            pltpu.VMEM((LAYERS, 6 * HEAD, WIDE), bf16),
            pltpu.VMEM((LAYERS, HEAD, WIDE), bf16),
            pltpu.VMEM((LAYERS, 2, LANES, WIDE), bf16),
            pltpu.VMEM((LAYERS, ROWS, 32, LANES), f32),
            pltpu.VMEM((LAYERS, 8, ROWS, 6 * HEAD), bf16),
            pltpu.VMEM((LAYERS, 7, ROWS, 6 * HEAD), bf16),
            pltpu.VMEM((LAYERS, 8, 1, LANES), f32),
            pltpu.VMEM((LAYERS, 7, 1, LANES), f32),
            pltpu.VMEM((LAYERS, 8, 16, LANES), bf16),
            pltpu.VMEM((LAYERS, 64, 16, LANES), bf16),
            pltpu.VMEM((LAYERS, 63, 16, LANES), bf16),
            pltpu.VMEM((LAYERS, 16, LANES), bf16),
            pltpu.VMEM((LAYERS, 64, 16, LANES), bf16),
        ]
        + [pltpu.VMEM((ROWS, LANES), f32)] * 6
        + [dma((8,)), dma((7,))]
        + [dma((LAYERS,))] * 10
        + [pltpu.SemaphoreType.REGULAR],
        compiler_params=pltpu.CompilerParams(
            collective_id=0, has_side_effects=True, vmem_limit_bytes=67043328
        ),
        name="blocks",
    )(tokens, norm_gain, *flat, decay_base, group_gain, output_proj, state.reshape(LAYERS, ROWS, 32, LANES))
    return (current, updated.reshape(LAYERS, ROWS, 1, HEAD * HEAD))


def solution(mesh):
    return jax.shard_map(
        shards,
        mesh=mesh,
        in_specs=(
            P(None, "dp"),
            P(None, "dp"),
            P(None, "dp", "tp"),
            P(None, "dp", "tp"),
            P(None, "dp", "tp"),
            P(None, "dp", "tp"),
            P(None, "dp", "tp"),
            P(None, "dp", "tp"),
            P(None, "tp"),
            P(None, "tp"),
            P(None, "tp", "dp"),
            P(None, "dp", "tp", None),
        ),
        out_specs=(P(None, "dp"), P(None, "dp", "tp", None)),
        check_vma=False,
    )
```

time: 180 us -> 75 us (0.42); the launches traced: 178 us -> 74.8 us
  Pallas kernels: 0 us -> 70.2 us
  waiting for transfers between devices: 64 us -> 0 us
  starting transfers between devices: 56.3 us -> 0 us
  local copies, waits for them, and re-layouts: 34.6 us -> 3.93 us
  other arithmetic: 12.4 us -> 0 us
  matrix products: 9.27 us -> 0 us
    pallas_call x0 -> x1, Pallas kernels: none -> 70.2 us  [shards(): pl.pallas_call(body, out_shape=(jax.ShapeDtypeStruct((256, WIDE), bf16),...]
    all_to_all x8 -> x0, waiting for transfers between devices: 64 us -> none  [the longest x4 36.5 us: sent_and_summed(): blocks = lax.all_to_all(cut_along(x, dim, peers), axis, 0, 0, tiled=True)]
    all_to_all x8 -> x0, starting transfers between devices: 56.3 us -> none  [the longest x4 34.4 us: sent_and_summed(): blocks = lax.all_to_all(cut_along(x, dim, peers), axis, 0, 0, tiled=True)]
    dot_general x18 -> x0, matrix products: 9.27 us -> none  [the longest x2 3.48 us: recurrence(): jnp.einsum('bhvk,bhk->bhv', state_block, -unit_key, precision=lax.Precisi...]
    unnamed x54 -> x2, local copies, waits for them, and re-layouts: 13 us -> 3.93 us
    mul x10 -> x0, local copies, waits for them, and re-layouts: 8.91 us -> none  [the longest x4 3.03 us: recurrence(): state_block * forget[:, :, None, :]]
    add x1 -> x0, other arithmetic: 4.23 us -> none  [recurrence(): state_block * forget[:, :, None, :]]
    slice x3 -> x0, local copies, waits for them, and re-layouts: 3.5 us -> none  [the longest x1 3.46 us: shards(): state[section_index].reshape(local_rows, local_heads, HEAD, HEAD)]
  transfers between devices with their start and end apart: 8 -> 0, of which waited for: 8 -> 0; matrix products, arithmetic and copies ran while one was open for 13% -> 0% of each run, Pallas kernels for 0% -> 0%
where the time goes in v1:
time: 75 us; the launch traced here: 74.8 us
  Pallas kernels  70.2 us (94%)
  local copies, waits for them, and re-layouts  3.93 us (5%)
    pallas_call x1, Pallas kernels, shards(): pl.pallas_call(body, out_shape=(jax.ShapeDtypeStruct((256, WIDE), bf16),...  70.2 us
    unnamed x2, local copies, waits for them, and re-layouts  3.93 us

profile of v1, /device:TPU:1, one launch (start us, length us, event | category | flops | bytes accessed | tf_op | source)
XLA Modules:
  0.0 74.8 jit_solution(4377868495468679857)
XLA Ops:
  0.6 70.2 %blocks.1 = (bf16[256,512]{1,0:T(8,128)(2,1)}, f32[2,32,32,128]{3,2,1,0:T(8,128)}) custom-call(bf16[256,512]{1,0:T(8,128)(2,1)} %tokens_ref.1, f32[2,512]{1,0:T(2,128)} %gain_ref.1, bf16[2,64,512]{2,1,0:T(8,128)(2,1)} %bitcast.10, bf16[2,64,512]{2,1,0:T(8,128)(2,1)} %bitcast.11, bf16[2,64,512]{2,1,0:T(8,128)(2,1)} %bitcast.12, bf16[2,64,512]{2,1,0:T(8,128)(2,1)} %bitcast.13, ...), custom_call_target="tpu_custom_call" | custom-call | tf_op jit(solution)/shard_map/blocks/pallas_call | solution.py:355
  70.8 1.7 %copy.17 = bf16[256,512]{1,0:T(8,128)(2,1)} copy(bf16[256,512]{1,0:T(8,128)(2,1)} %get-tuple-element.10) | data formatting | bytes 524288
  72.5 2.3 %copy.18 = f32[2,32,1,4096]{3,2,1,0:T(1,128)} copy(f32[2,32,1,4096]{3,2,1,0:T(1,128)} %bitcast.9) | data formatting | bytes 2097152

commit v2 on v1

v2 whole, which is shorter than its diff:
```python
import jax
import jax.numpy as jnp
from jax import lax
from jax.experimental import pallas as pl
from jax.experimental.pallas import tpu as pltpu
from jax.sharding import PartitionSpec as P

D = 4096
HEAD = 64
LAYERS = 2
ROWS = 32
WIDE = 512
LANES = 128

norm_floor = 0.1
group_floor = 0.5

MESH = pl.DeviceIdType.MESH
RING8 = (4, 3, 5, 2, 6, 1, 7)
TP_OFFSETS = sorted(
    ((a, b) for a in range(8) for b in range(8) if (a, b) != (0, 0)),
    key=lambda ab: -(min(ab[0], 8 - ab[0]) + min(ab[1], 8 - ab[1])),
)


def iota(shape, dim):
    return lax.broadcasted_iota(jnp.int32, shape, dim)


def two_terms(x):
    high = x.astype(jnp.bfloat16)
    low = (x - high.astype(jnp.float32)).astype(jnp.bfloat16)
    return jnp.concatenate([high, low], axis=1)


def dot(a, b):
    return jnp.dot(a, b, preferred_element_type=jnp.float32)


def wait_for(ref, sem):
    pltpu.make_async_copy(ref, ref, sem).wait()


def body(
    tokens_ref,
    gain_in,
    w0,
    w1,
    w2,
    w3,
    w4,
    w5,
    decay_in,
    group_in,
    out_proj_ref,
    state_ref,
    next_ref,
    new_state_ref,
    tokens,
    first_weights,
    weights,
    wout,
    gains,
    decay_ref,
    group_ref,
    residue,
    state,
    part_send,
    part_recv,
    sq_send,
    sq_recv,
    out_send,
    out_recv,
    share,
    x_all,
    x_last,
    vec_g,
    vec_f,
    vec_s,
    vec_u,
    vec_v,
    read_rows,
    load_sem,
    late_sem,
    part_sem,
    sq_sem,
    out_sem,
    x_sem,
    gain_sem,
    residue_sem,
    wout_sem,
    wout_core_sem,
    ring_sem,
    core_sem,
    last_sem,
    row_sem,
    plane_sem,
):
    tp = lax.axis_index("tp")
    dp = lax.axis_index("dp")
    z = tp // 8
    y = lax.rem(tp, 8)
    x = dp // 2
    core = lax.rem(dp, 2)
    dp_peers = [(tp, lax.rem(dp + o, 8)) for o in RING8]
    y_peers = [(z * 8 + lax.rem(y + o, 8), dp) for o in RING8]
    z_peers = [(lax.rem(z + o, 8) * 8 + y, dp) for o in RING8]
    tp_peers = [(lax.rem(z + a, 8) * 8 + lax.rem(y + b, 8), dp) for a, b in TP_OFFSETS]
    right, far, left = (lax.rem(x + o, 4) * 2 + core for o in (1, 2, 3))
    partner = x * 2 + (1 - core)
    owns_columns = dp == z
    half_row = lax.rem(y, 2)
    column = y // 2

    def remote(src, dst, sems, peer):
        copy = pltpu.make_async_remote_copy(
            src_ref=src, dst_ref=dst, send_sem=sems[0], recv_sem=sems[1], device_id=peer, device_id_type=MESH
        )
        copy.start()
        return copy

    barrier = pltpu.get_barrier_semaphore()
    for peer in dp_peers + y_peers + z_peers:
        pl.semaphore_signal(barrier, inc=1, device_id=peer, device_id_type=MESH)

    def load(src, dst, sem):
        copy = pltpu.make_async_copy(src, dst, sem)
        copy.start()
        return copy

    tokens_load = load(tokens_ref, tokens, load_sem.at[0])
    gain_load = load(gain_in, gains.at[dp], load_sem.at[7])
    small_loads = [load(decay_in, decay_ref, load_sem.at[8]), load(group_in, group_ref, load_sem.at[9])]
    projections = (w0, w1, w2, w3, w4, w5)
    first_loads = [
        load(w.at[0], first_weights.at[pl.ds(n * HEAD, HEAD)], load_sem.at[n + 1]) for n, w in enumerate(projections)
    ]
    wout_loads = [load(out_proj_ref.at[b], wout.at[b, dp], late_sem.at[7 + b]) for b in range(LAYERS)]
    state_load = load(state_ref, state, late_sem.at[0])
    weight_loads = [
        load(w.at[1], weights.at[dp, pl.ds(n * HEAD, HEAD)], late_sem.at[n + 1]) for n, w in enumerate(projections)
    ]

    lane = iota((ROWS, LANES), 1)
    row = iota((ROWS, LANES), 0)
    low_half = lane < HEAD
    eye = (lane == row).astype(jnp.float32)
    pick = (lane % HEAD) // 2 == row
    pick_own = lane % HEAD == 2 * row + lane // HEAD
    ones = jnp.full((2 * LANES, LANES), 1.0, jnp.bfloat16)
    k_of = iota((2 * LANES, LANES), 0)
    l_of = iota((2 * LANES, LANES), 1)
    by_parity = ((k_of // HEAD) % 2 == l_of % 2).astype(jnp.float32).astype(jnp.bfloat16)
    by_half = ((k_of // HEAD) % 2 == l_of // HEAD).astype(jnp.float32).astype(jnp.bfloat16)

    waits = []

    def first_parts():
        columns = [tokens[:, c * LANES : (c + 1) * LANES].astype(jnp.float32) for c in range(4)]
        squares = columns[0] * columns[0]
        for c in columns[1:]:
            squares = squares + c * c
        totals = dot(two_terms(squares), ones)
        for o in range(8):
            sq_send[o] = jnp.sum(totals[o * ROWS : (o + 1) * ROWS] * eye, axis=0, keepdims=True)
        gain_load.wait()
        normed = jnp.concatenate(
            [(c * gains[dp, 0:1, n * LANES : (n + 1) * LANES]).astype(jnp.bfloat16) for n, c in enumerate(columns)],
            axis=1,
        )
        for copy in first_loads:
            copy.wait()
        part = lax.dot_general(
            normed, first_weights[...], (((1,), (1,)), ((), ())), preferred_element_type=jnp.float32
        ).astype(jnp.bfloat16)
        for o in range(8):
            part_send[o] = part[o * ROWS : (o + 1) * ROWS]

    def send_parts():
        for i, peer in enumerate(dp_peers):
            remote(part_send.at[peer[1]], part_recv.at[i], (part_sem.at[0], part_sem.at[1]), peer)
            remote(sq_send.at[peer[1]], sq_recv.at[i], (sq_sem.at[0], sq_sem.at[1]), peer)
        waits.append((part_recv, part_sem.at[0]))
        waits.append((sq_recv, sq_sem.at[0]))

    def first_projected():
        wait_for(sq_recv, sq_sem.at[1])
        square = sq_send[dp]
        for i in range(7):
            square = square + sq_recv[i]
        inv = lax.rsqrt(jnp.sum(square * eye, axis=1, keepdims=True) / D + norm_floor)
        wait_for(part_recv, part_sem.at[1])
        total = part_send[dp].astype(jnp.float32)
        for i in range(7):
            total = total + part_recv[i].astype(jnp.float32)
        return total * inv

    def second_projected():
        squares = jnp.zeros((ROWS, LANES), jnp.float32)
        total = jnp.zeros((ROWS, 6 * HEAD), jnp.float32)
        for d in range(8):
            pieces = []
            for c in range(4):
                at = (d * 4 + c) * 2
                piece = jnp.concatenate([x_all[at], x_all[at + 1]], axis=0).astype(jnp.float32)
                squares = squares + piece * piece
                pieces.append((piece * gains[d, 1:2, c * LANES : (c + 1) * LANES]).astype(jnp.bfloat16))
            total = total + lax.dot_general(
                jnp.concatenate(pieces, axis=1),
                weights[d],
                (((1,), (1,)), ((), ())),
                preferred_element_type=jnp.float32,
            )
        inv = lax.rsqrt(jnp.sum(squares, axis=1, keepdims=True) / D + norm_floor)
        return total * inv

    def mix(b, projected):
        heads = projected.astype(jnp.bfloat16).astype(jnp.float32)
        both = []
        for n in range(3):
            tile = heads[:, n * LANES : (n + 1) * LANES]
            turned = pltpu.roll(tile, HEAD, 1)
            both.append(jnp.where(low_half, tile, turned))
            both.append(jnp.where(low_half, turned, tile))
        recept, keys, values, decay_part, rate_part, gate_part = both
        base = decay_ref[b : b + 1, :]
        decay = jnp.concatenate([base, base], axis=1) + decay_part
        forget = jnp.exp(-jnp.exp(-jax.nn.softplus(-decay) - 0.5))
        learn = jax.nn.sigmoid(rate_part)
        norm = lax.rsqrt(0.5 * jnp.sum(keys * keys, axis=1, keepdims=True) + 1.0)
        scaled = keys * learn
        with_scaled = 0.5 * jnp.sum(scaled * recept, axis=1, keepdims=True)
        unit = keys * norm
        vec_g[...] = forget * recept - (with_scaled * norm) * unit
        vec_f[...] = forget
        vec_s[...] = scaled
        vec_u[...] = unit * norm
        vec_v[...] = values
        for c in range(4):
            terms = jnp.concatenate([state[b, r] * vec_g[r : r + 1, :] for r in range(c * 8, c * 8 + 8)], axis=0)
            sums = dot(two_terms(terms), by_parity)
            for r in range(8):
                at = c * 8 + r
                chosen = jnp.where(pick, sums[r * ROWS : (r + 1) * ROWS], 0.0)
                read_rows[at : at + 1, :] = jnp.sum(chosen, axis=0, keepdims=True)
        read = read_rows[...] + values * with_scaled
        centre = read - jnp.mean(read, axis=1, keepdims=True)
        normal = centre * lax.rsqrt(jnp.mean(centre * centre, axis=1, keepdims=True) + group_floor)
        gain = group_ref[b : b + 1, :]
        return (normal * jnp.concatenate([gain, gain], axis=1) * jax.nn.sigmoid(gate_part)).astype(jnp.bfloat16)

    def project_out(b, mixed):
        rows = mixed[:, :HEAD]
        for d in range(8):
            term = dot(rows, wout[b, d]).astype(jnp.bfloat16)
            for c in range(4):
                for half in range(2):
                    out_send[b, (d * 4 + c) * 2 + half] = term[
                        half * 16 : (half + 1) * 16, c * LANES : (c + 1) * LANES
                    ]

    def send_out(b):
        for i, peer in enumerate(tp_peers):
            remote(out_send.at[b, peer[0]], out_recv.at[b, i], (out_sem.at[b], out_sem.at[2 + b]), peer)
        waits.append((out_recv.at[b], out_sem.at[b]))

    def update_state(b):
        for c in range(4):
            terms = jnp.concatenate(
                [
                    jnp.where(pick_own, vec_v[r : r + 1, :], 0.0) - state[b, r] * vec_u[r : r + 1, :]
                    for r in range(c * 8, c * 8 + 8)
                ],
                axis=0,
            )
            sums = dot(two_terms(terms), by_half)
            for r in range(8):
                at = c * 8 + r
                new_state_ref[b, at] = (
                    state[b, at] * vec_f[at : at + 1, :] + sums[r * ROWS : (r + 1) * ROWS] * vec_s[at : at + 1, :]
                )

    def finish_share(b, mine):
        wait_for(out_recv.at[b], out_sem.at[2 + b])
        parts = [out_send[b, tp].astype(jnp.float32)] + [jnp.zeros((16, LANES), jnp.float32)] * 3
        for i in range(63):
            parts[(i + 1) % 4] = parts[(i + 1) % 4] + out_recv[b, i].astype(jnp.float32)
        total = (parts[0] + parts[1]) + (parts[2] + parts[3])
        share[b] = (mine.astype(jnp.float32) + total).astype(jnp.bfloat16)

    def gather_wout(b):
        wout_loads[b].wait()
        for peer in (far, right, left):
            remote(wout.at[b, dp], wout.at[b, dp], (wout_sem.at[b], wout_sem.at[2 + b]), (tp, peer))
        remote(wout.at[b, dp], wout.at[b, dp], (wout_core_sem.at[b], wout_core_sem.at[2 + b]), (tp, partner))
        waits.append((wout.at[b, pl.ds(0, 3)], wout_sem.at[b]))

    def pass_wout(b):
        wait_for(wout.at[b, pl.ds(0, 3)], wout_sem.at[2 + b])
        for peer in (far, right, left):
            remote(
                wout.at[b, peer], wout.at[b, peer], (wout_core_sem.at[b], wout_core_sem.at[2 + b]), (tp, partner)
            )
        waits.append((wout.at[b, pl.ds(0, 4)], wout_core_sem.at[b]))

    half_rows = 3 * HEAD

    def gather_weights():
        for copy in weight_loads:
            copy.wait()
        mine = weights.at[dp]
        remote(mine, mine, (ring_sem.at[0], ring_sem.at[4]), (tp, right))
        remote(mine, mine, (ring_sem.at[1], ring_sem.at[5]), (tp, left))
        remote(mine, mine, (core_sem.at[0], core_sem.at[1]), (tp, partner))
        waits.append((mine, ring_sem.at[0]))
        waits.append((mine, ring_sem.at[1]))

    def pass_weights():
        first, second = pl.ds(0, half_rows), pl.ds(half_rows, half_rows)
        from_left, from_right = weights.at[left], weights.at[right]
        wait_for(from_left, ring_sem.at[4])
        remote(weights.at[left, first], weights.at[left, first], (ring_sem.at[2], ring_sem.at[6]), (tp, right))
        wait_for(from_right, ring_sem.at[5])
        remote(weights.at[right, second], weights.at[right, second], (ring_sem.at[3], ring_sem.at[7]), (tp, left))
        remote(from_left, from_left, (core_sem.at[0], core_sem.at[1]), (tp, partner))
        remote(from_right, from_right, (core_sem.at[0], core_sem.at[1]), (tp, partner))
        waits.append((weights.at[left, first], ring_sem.at[2]))
        waits.append((weights.at[left, first], ring_sem.at[3]))

    def end_weights():
        wait_for(weights.at[far, pl.ds(0, half_rows)], ring_sem.at[6])
        wait_for(weights.at[far, pl.ds(0, half_rows)], ring_sem.at[7])
        remote(weights.at[far], weights.at[far], (core_sem.at[0], core_sem.at[1]), (tp, partner))
        waits.append((weights.at[pl.ds(0, 4)], core_sem.at[0]))
        wait_for(weights.at[pl.ds(0, 4)], core_sem.at[1])

    tokens_load.wait()
    first_parts()
    pl.semaphore_wait(barrier, 21)
    send_parts()
    gather_wout(0)
    for peer in dp_peers:
        remote(gains.at[dp], gains.at[dp], (gain_sem.at[0], gain_sem.at[1]), peer)
    waits.append((gains.at[pl.ds(0, 7)], gain_sem.at[0]))
    at_column = pl.ds(pl.multiple_of(column * LANES, LANES), LANES)

    def at_rows(owner):
        return pl.ds(pl.multiple_of(owner * ROWS + half_row * 16, 16), 16)

    @pl.when(owns_columns)
    def _():
        for peer in dp_peers:
            remote(tokens.at[at_rows(peer[1]), at_column], residue, (residue_sem.at[0], residue_sem.at[1]), peer)
        residue[...] = tokens[at_rows(dp), at_column]

    for peer in z_peers:
        pl.semaphore_signal(row_sem, inc=1, device_id=peer, device_id_type=MESH)
    gather_weights()
    pass_wout(0)
    projected = first_projected()
    for copy in small_loads + [state_load]:
        copy.wait()
    mixed = mix(0, projected)
    pl.semaphore_wait(row_sem, 7)
    for peer in dp_peers:
        pl.semaphore_signal(plane_sem, inc=1, device_id=peer, device_id_type=MESH)
    wait_for(wout.at[0, pl.ds(0, 4)], wout_core_sem.at[2])
    project_out(0, mixed)
    send_out(0)
    update_state(0)

    @pl.when(jnp.logical_not(owns_columns))
    def _():
        wait_for(residue, residue_sem.at[1])

    finish_share(0, residue[...])
    x_all[tp] = share[0]
    for peer in tp_peers:
        remote(share.at[0], x_all.at[tp], (x_sem.at[0], x_sem.at[1]), peer)
    waits.append((x_all.at[pl.ds(0, 63)], x_sem.at[0]))
    pass_weights()
    gather_wout(1)
    pass_wout(1)
    wait_for(gains.at[pl.ds(0, 7)], gain_sem.at[1])
    pl.semaphore_wait(plane_sem, 7)
    end_weights()
    wait_for(wout.at[1, pl.ds(0, 4)], wout_core_sem.at[3])
    wait_for(x_all.at[pl.ds(0, 63)], x_sem.at[1])

    project_out(1, mix(1, second_projected()))
    send_out(1)
    update_state(1)
    finish_share(1, share[0])
    slot = (dp * 2 + half_row) * 4 + column

    @pl.when(jnp.logical_not(owns_columns))
    def _():
        remote(share.at[1], x_last.at[slot], (last_sem.at[2], last_sem.at[1]), (tp, z))

    @pl.when(owns_columns)
    def _():
        load(share.at[1], x_last.at[slot], last_sem.at[1])

    for peer in tp_peers:
        remote(share.at[1], x_last.at[slot], (last_sem.at[0], last_sem.at[1]), (peer[0], z))
    waits.append((x_last.at[pl.ds(0, 63)], last_sem.at[0]))
    wait_for(x_last, last_sem.at[1])
    for g in range(16):
        for c in range(4):
            next_ref[g * 16 : (g + 1) * 16, c * LANES : (c + 1) * LANES] = x_last[g * 4 + c]

    @pl.when(jnp.logical_not(owns_columns))
    def _():
        wait_for(share.at[1], last_sem.at[2])

    @pl.when(owns_columns)
    def _():
        wait_for(x_last.at[pl.ds(0, 7)], residue_sem.at[0])

    for ref, sem in waits:
        wait_for(ref, sem)


def write_out(next_ref, state_ref, next_out, state_out, sems):
    copies = [
        pltpu.make_async_copy(src, dst, sems.at[n])
        for n, (src, dst) in enumerate(((state_ref, state_out), (next_ref, next_out)))
    ]
    for copy in copies:
        copy.start()
    for copy in copies:
        copy.wait()


def shards(
    tokens,
    norm_gain,
    receptance,
    key_proj,
    value_proj,
    decay_proj,
    rate_proj,
    gate_proj,
    decay_base,
    group_gain,
    output_proj,
    state,
):
    flat = [jnp.swapaxes(w, 1, 2) for w in (receptance, key_proj, value_proj, decay_proj, rate_proj, gate_proj)]
    remote = pl.BlockSpec(memory_space=pltpu.HBM)
    local = pl.BlockSpec(memory_space=pltpu.VMEM)
    f32, bf16 = jnp.float32, jnp.bfloat16
    dma = pltpu.SemaphoreType.DMA

    current, updated = pl.pallas_call(
        body,
        out_shape=(
            pltpu.VMEM((256, WIDE), bf16),
            pltpu.VMEM((LAYERS, ROWS, 32, LANES), f32),
        ),
        in_specs=[remote] * 12,
        out_specs=(local, local),
        scratch_shapes=[
            pltpu.VMEM((256, WIDE), bf16),
            pltpu.VMEM((6 * HEAD, WIDE), bf16),
            pltpu.VMEM((8, 6 * HEAD, WIDE), bf16),
            pltpu.VMEM((LAYERS, 8, HEAD, WIDE), bf16),
            pltpu.VMEM((8, LAYERS, WIDE), f32),
            pltpu.VMEM((LAYERS, HEAD), f32),
            pltpu.VMEM((LAYERS, HEAD), f32),
            pltpu.VMEM((16, LANES), bf16),
            pltpu.VMEM((LAYERS, ROWS, 32, LANES), f32),
            pltpu.VMEM((8, ROWS, 6 * HEAD), bf16),
            pltpu.VMEM((7, ROWS, 6 * HEAD), bf16),
            pltpu.VMEM((8, 1, LANES), f32),
            pltpu.VMEM((7, 1, LANES), f32),
            pltpu.VMEM((LAYERS, 64, 16, LANES), bf16),
            pltpu.VMEM((LAYERS, 63, 16, LANES), bf16),
            pltpu.VMEM((LAYERS, 16, LANES), bf16),
            pltpu.VMEM((64, 16, LANES), bf16),
            pltpu.VMEM((64, 16, LANES), bf16),
        ]
        + [pltpu.VMEM((ROWS, LANES), f32)] * 6
        + [dma((10,)), dma((9,)), dma((2,)), dma((2,)), dma((4,)), dma((2,)), dma((2,)), dma((2,))]
        + [dma((4,)), dma((4,)), dma((8,)), dma((2,)), dma((3,))]
        + [pltpu.SemaphoreType.REGULAR] * 2,
        compiler_params=pltpu.CompilerParams(
            collective_id=0, has_side_effects=True, vmem_limit_bytes=32 * 1024 * 1024
        ),
        name="blocks",
    )(
        *[
            pltpu.with_memory_space_constraint(a, pltpu.HBM)
            for a in (
                tokens,
                norm_gain,
                *flat,
                decay_base,
                group_gain,
                output_proj,
                state.reshape(LAYERS, ROWS, 32, LANES),
            )
        ]
    )
    current, updated = pl.pallas_call(
        write_out,
        out_shape=(
            jax.ShapeDtypeStruct((256, WIDE), bf16),
            jax.ShapeDtypeStruct((LAYERS, ROWS, 32, LANES), f32),
        ),
        in_specs=[local, local],
        out_specs=(remote, remote),
        scratch_shapes=[dma((2,))],
        name="write_out",
    )(*[pltpu.with_memory_space_constraint(a, pltpu.VMEM) for a in (current, updated)])
    return (current, updated.reshape(LAYERS, ROWS, 1, HEAD * HEAD))


def solution(mesh):
    return jax.shard_map(
        shards,
        mesh=mesh,
        in_specs=(
            P(None, "dp"),
            P(None, "dp"),
            P(None, "dp", "tp"),
            P(None, "dp", "tp"),
            P(None, "dp", "tp"),
            P(None, "dp", "tp"),
            P(None, "dp", "tp"),
            P(None, "dp", "tp"),
            P(None, "tp"),
            P(None, "tp"),
            P(None, "tp", "dp"),
            P(None, "dp", "tp", None),
        ),
        out_specs=(P(None, "dp"), P(None, "dp", "tp", None)),
        check_vma=False,
    )
```

time: 75 us -> 67.9 us (0.905)
  local copies, waits for them, and re-layouts: 3.93 us -> 0 us
  Pallas kernels: 70.2 us -> 67.1 us
    unnamed x2 -> x0, local copies, waits for them, and re-layouts: 3.93 us -> none
    pallas_call x1 -> x2, Pallas kernels: 70.2 us -> 67.1 us  [the longest x1 66.1 us: shards(): pl.pallas_call(body, out_shape=(pltpu.VMEM((256, WIDE), bf16), pltpu.VMEM...]
where the time goes in v2:
time: 67.9 us; the launch traced here: 67.8 us
  Pallas kernels  67.1 us (99%)
    pallas_call x1, Pallas kernels, shards(): pl.pallas_call(body, out_shape=(pltpu.VMEM((256, WIDE), bf16), pltpu.VMEM...  66.1 us

profile of v2, /device:TPU:1, one launch (start us, length us, event | category | flops | bytes accessed | tf_op | source)
XLA Modules:
  0.0 67.8 jit_solution(16129393747956264279)
XLA Ops:
  0.6 66.1 %blocks.1 = (bf16[256,512]{1,0:T(8,128)(2,1)S(1)}, f32[2,32,32,128]{3,2,1,0:T(8,128)S(1)}) custom-call(bf16[256,512]{1,0:T(8,128)(2,1)} %tokens_ref.1, f32[2,512]{1,0:T(2,128)} %gain_in.1, bf16[2,64,512]{2,1,0:T(8,128)(2,1)} %bitcast.9, bf16[2,64,512]{2,1,0:T(8,128)(2,1)} %bitcast.10, bf16[2,64,512]{2,1,0:T(8,128)(2,1)} %bitcast.11, ...), custom_call_target="tpu_custom_call" | custom-call | tf_op jit(solution)/shard_map/blocks/pallas_call | solution.py:455
  66.7 1.1 %write_out.1 = (bf16[256,512]{1,0:T(8,128)(2,1)}, f32[2,32,32,128]{3,2,1,0:T(8,128)}) custom-call(bf16[256,512]{1,0:T(8,128)(2,1)S(1)} %get-tuple-element.6.next_ref, f32[2,32,32,128]{3,2,1,0:T(8,128)S(1)} %get-tuple-element.7.state_ref), custom_call_target="tpu_custom_call" | custom-call | tf_op jit(solution)/shard_map/write_out/pallas_call | solution.py:505

commit v3 on v2

--- a/solution.py
+++ b/solution.py
@@ -66,6 +66,8 @@
     residue,
     state,
     part_send,
+    part_core,
+    part_sum,
     part_recv,
     sq_send,
     sq_recv,
@@ -82,6 +84,7 @@
     read_rows,
     load_sem,
     late_sem,
+    pair_sem,
     part_sem,
     sq_sem,
     out_sem,
@@ -93,6 +96,8 @@
     ring_sem,
     core_sem,
     last_sem,
+    near_sem,
+    line_sem,
     row_sem,
     plane_sem,
 ):
@@ -103,7 +108,6 @@
     x = dp // 2
     core = lax.rem(dp, 2)
     dp_peers = [(tp, lax.rem(dp + o, 8)) for o in RING8]
-    y_peers = [(z * 8 + lax.rem(y + o, 8), dp) for o in RING8]
     z_peers = [(lax.rem(z + o, 8) * 8 + y, dp) for o in RING8]
     tp_peers = [(lax.rem(z + a, 8) * 8 + lax.rem(y + b, 8), dp) for a, b in TP_OFFSETS]
     right, far, left = (lax.rem(x + o, 4) * 2 + core for o in (1, 2, 3))
@@ -119,9 +123,17 @@
         copy.start()
         return copy
 
+    def beside(o):
+        return [(z * 8 + lax.rem(y + k, 8), dp) for k in (o, 8 - o)] + [
+            (lax.rem(z + k, 8) * 8 + y, dp) for k in (o, 8 - o)
+        ]
+
+    def tell(sem, peers):
+        for peer in peers:
+            pl.semaphore_signal(sem, inc=1, device_id=peer, device_id_type=MESH)
+
     barrier = pltpu.get_barrier_semaphore()
-    for peer in dp_peers + y_peers + z_peers:
-        pl.semaphore_signal(barrier, inc=1, device_id=peer, device_id_type=MESH)
+    tell(barrier, dp_peers + beside(1))
 
     def load(src, dst, sem):
         copy = pltpu.make_async_copy(src, dst, sem)
@@ -177,11 +189,22 @@
             part_send[o] = part[o * ROWS : (o + 1) * ROWS]
 
     def send_parts():
+        for chip in range(4):
+            remote(part_send.at[chip * 2 + 1 - core], part_core.at[chip], (pair_sem.at[0], pair_sem.at[1]), (tp, partner))
         for i, peer in enumerate(dp_peers):
-            remote(part_send.at[peer[1]], part_recv.at[i], (part_sem.at[0], part_sem.at[1]), peer)
             remote(sq_send.at[peer[1]], sq_recv.at[i], (sq_sem.at[0], sq_sem.at[1]), peer)
+        waits.append((part_core, pair_sem.at[0]))
+        waits.append((sq_recv, sq_sem.at[0]))
+
+    def send_pair_sums():
+        wait_for(part_core, pair_sem.at[1])
+        for chip in range(4):
+            both = part_send[chip * 2 + core].astype(jnp.float32) + part_core[chip].astype(jnp.float32)
+            part_sum[chip] = both.astype(jnp.bfloat16)
+        for i, o in enumerate((2, 1, 3)):
+            chip = lax.rem(x + o, 4)
+            remote(part_sum.at[chip], part_recv.at[i], (part_sem.at[0], part_sem.at[1]), (tp, chip * 2 + core))
         waits.append((part_recv, part_sem.at[0]))
-        waits.append((sq_recv, sq_sem.at[0]))
 
     def first_projected():
         wait_for(sq_recv, sq_sem.at[1])
@@ -190,15 +213,17 @@
             square = square + sq_recv[i]
         inv = lax.rsqrt(jnp.sum(square * eye, axis=1, keepdims=True) / D + norm_floor)
         wait_for(part_recv, part_sem.at[1])
-        total = part_send[dp].astype(jnp.float32)
-        for i in range(7):
+        total = part_sum[x].astype(jnp.float32)
+        for i in range(3):
             total = total + part_recv[i].astype(jnp.float32)
         return total * inv
 
     def second_projected():
         squares = jnp.zeros((ROWS, LANES), jnp.float32)
-        total = jnp.zeros((ROWS, 6 * HEAD), jnp.float32)
-        for d in range(8):
+        total = jnp.zeros((6 * HEAD, ROWS), jnp.float32)
+        for a in RING8 + (0,):
+            d = lax.rem(z + 8 - a, 8)
+            wait_for(x_all.at[pl.ds(0, 8 if a else 7)], x_sem.at[a])
             pieces = []
             for c in range(4):
                 at = (d * 4 + c) * 2
@@ -206,13 +231,13 @@
                 squares = squares + piece * piece
                 pieces.append((piece * gains[d, 1:2, c * LANES : (c + 1) * LANES]).astype(jnp.bfloat16))
             total = total + lax.dot_general(
+                weights[d],
                 jnp.concatenate(pieces, axis=1),
-                weights[d],
                 (((1,), (1,)), ((), ())),
                 preferred_element_type=jnp.float32,
             )
         inv = lax.rsqrt(jnp.sum(squares, axis=1, keepdims=True) / D + norm_floor)
-        return total * inv
+        return total.T * inv
 
     def mix(b, projected):
         heads = projected.astype(jnp.bfloat16).astype(jnp.float32)
@@ -249,20 +274,21 @@
         gain = group_ref[b : b + 1, :]
         return (normal * jnp.concatenate([gain, gain], axis=1) * jax.nn.sigmoid(gate_part)).astype(jnp.bfloat16)
 
-    def project_out(b, mixed):
-        rows = mixed[:, :HEAD]
-        for d in range(8):
+    own_columns = [lax.rem(x + o, 4) * 2 + core for o in (2, 1, 3, 0)]
+    other_columns = [lax.rem(x + o, 4) * 2 + (1 - core) for o in (2, 1, 3, 0)]
+
+    def project_out(b, rows, blocks):
+        for d in blocks:
             term = dot(rows, wout[b, d]).astype(jnp.bfloat16)
             for c in range(4):
                 for half in range(2):
-                    out_send[b, (d * 4 + c) * 2 + half] = term[
+                    out_send[b, d * 8 + c * 2 + half] = term[
                         half * 16 : (half + 1) * 16, c * LANES : (c + 1) * LANES
                     ]
 
     def send_out(b):
-        for i, peer in enumerate(tp_peers):
-            remote(out_send.at[b, peer[0]], out_recv.at[b, i], (out_sem.at[b], out_sem.at[2 + b]), peer)
-        waits.append((out_recv.at[b], out_sem.at[b]))
+        for peer in tp_peers:
+            remote(out_send.at[b, peer[0]], out_recv.at[b, tp], (out_sem.at[b], out_sem.at[2 + b]), peer)
 
     def update_state(b):
         for c in range(4):
@@ -281,64 +307,106 @@
                 )
 
     def finish_share(b, mine):
-        wait_for(out_recv.at[b], out_sem.at[2 + b])
-        parts = [out_send[b, tp].astype(jnp.float32)] + [jnp.zeros((16, LANES), jnp.float32)] * 3
-        for i in range(63):
-            parts[(i + 1) % 4] = parts[(i + 1) % 4] + out_recv[b, i].astype(jnp.float32)
+        wait_for(out_recv.at[b, pl.ds(0, 63)], out_sem.at[2 + b])
+        waits.append((out_recv.at[b, pl.ds(0, 63)], out_sem.at[b]))
+        out_recv[b, tp] = out_send[b, tp]
+        parts = [out_recv[b, i].astype(jnp.float32) for i in range(4)]
+        for i in range(4, 64):
+            parts[i % 4] = parts[i % 4] + out_recv[b, i].astype(jnp.float32)
         total = (parts[0] + parts[1]) + (parts[2] + parts[3])
         share[b] = (mine.astype(jnp.float32) + total).astype(jnp.bfloat16)
 
-    def gather_wout(b):
-        wout_loads[b].wait()
+    def to_partner(b, owner):
+        there = wout.at[b, owner]
+        remote(there, there, (wout_core_sem.at[b], wout_core_sem.at[2 + b]), (tp, partner))
+
+    def gather_first_wout():
+        mine = out_proj_ref.at[0]
         for peer in (far, right, left):
-            remote(wout.at[b, dp], wout.at[b, dp], (wout_sem.at[b], wout_sem.at[2 + b]), (tp, peer))
-        remote(wout.at[b, dp], wout.at[b, dp], (wout_core_sem.at[b], wout_core_sem.at[2 + b]), (tp, partner))
-        waits.append((wout.at[b, pl.ds(0, 3)], wout_sem.at[b]))
-
-    def pass_wout(b):
-        wait_for(wout.at[b, pl.ds(0, 3)], wout_sem.at[2 + b])
+            remote(mine, wout.at[0, dp], (wout_sem.at[0], wout_sem.at[1]), (tp, peer))
+        remote(mine, wout.at[0, dp], (wout_core_sem.at[0], wout_core_sem.at[2]), (tp, partner))
+        waits.append((wout.at[0, pl.ds(0, 3)], wout_sem.at[0]))
+
+    def pass_first_wout():
+        wait_for(wout.at[0, pl.ds(0, 3)], wout_sem.at[1])
         for peer in (far, right, left):
-            remote(
-                wout.at[b, peer], wout.at[b, peer], (wout_core_sem.at[b], wout_core_sem.at[2 + b]), (tp, partner)
-            )
-        waits.append((wout.at[b, pl.ds(0, 4)], wout_core_sem.at[b]))
-
-    half_rows = 3 * HEAD
+            to_partner(0, peer)
+        waits.append((wout.at[0, pl.ds(0, 4)], wout_core_sem.at[0]))
+
+    def gather_second_wout():
+        mine = out_proj_ref.at[1]
+        remote(mine, wout.at[1, dp], (wout_sem.at[2], wout_sem.at[3]), (tp, left))
+        remote(mine, wout.at[1, dp], (wout_sem.at[4], wout_sem.at[5]), (tp, right))
+        remote(mine, wout.at[1, dp], (wout_core_sem.at[1], wout_core_sem.at[3]), (tp, partner))
+        waits.append((wout.at[1, 0], wout_sem.at[2]))
+        waits.append((wout.at[1, 0], wout_sem.at[4]))
+
+    def pass_second_wout():
+        from_right = wout.at[1, right]
+        wait_for(from_right, wout_sem.at[3])
+        remote(from_right, from_right, (wout_sem.at[6], wout_sem.at[7]), (tp, left))
+        to_partner(1, right)
+        wait_for(wout.at[1, left], wout_sem.at[5])
+        to_partner(1, left)
+        waits.append((wout.at[1, 0], wout_sem.at[6]))
+
+    def end_second_wout():
+        wait_for(wout.at[1, far], wout_sem.at[7])
+        to_partner(1, far)
+        waits.append((wout.at[1, pl.ds(0, 4)], wout_core_sem.at[1]))
+
+    halves = (pl.ds(0, 3 * HEAD), pl.ds(3 * HEAD, 3 * HEAD))
+
+    def half(owner, n):
+        return weights.at[owner, halves[n]]
+
+    def ring_send(owner, n, at, peer):
+        there = half(owner, n)
+        remote(there, there, (ring_sem.at[at], ring_sem.at[6 + at]), (tp, peer))
+        waits.append((half(0, 0), ring_sem.at[at]))
+
+    def core_send(owner):
+        there = weights.at[owner]
+        remote(there, there, (core_sem.at[0], core_sem.at[1]), (tp, partner))
 
     def gather_weights():
         for copy in weight_loads:
             copy.wait()
-        mine = weights.at[dp]
-        remote(mine, mine, (ring_sem.at[0], ring_sem.at[4]), (tp, right))
-        remote(mine, mine, (ring_sem.at[1], ring_sem.at[5]), (tp, left))
-        remote(mine, mine, (core_sem.at[0], core_sem.at[1]), (tp, partner))
-        waits.append((mine, ring_sem.at[0]))
-        waits.append((mine, ring_sem.at[1]))
+        ring_send(dp, 0, 0, right)
+        ring_send(dp, 1, 2, left)
+        ring_send(dp, 1, 1, right)
+        ring_send(dp, 0, 3, left)
+        core_send(dp)
 
     def pass_weights():
-        first, second = pl.ds(0, half_rows), pl.ds(half_rows, half_rows)
-        from_left, from_right = weights.at[left], weights.at[right]
-        wait_for(from_left, ring_sem.at[4])
-        remote(weights.at[left, first], weights.at[left, first], (ring_sem.at[2], ring_sem.at[6]), (tp, right))
-        wait_for(from_right, ring_sem.at[5])
-        remote(weights.at[right, second], weights.at[right, second], (ring_sem.at[3], ring_sem.at[7]), (tp, left))
-        remote(from_left, from_left, (core_sem.at[0], core_sem.at[1]), (tp, partner))
-        remote(from_right, from_right, (core_sem.at[0], core_sem.at[1]), (tp, partner))
-        waits.append((weights.at[left, first], ring_sem.at[2]))
-        waits.append((weights.at[left, first], ring_sem.at[3]))
+        wait_for(half(right, 1), ring_sem.at[8])
+        ring_send(right, 1, 5, left)
+        wait_for(half(left, 0), ring_sem.at[6])
+        ring_send(left, 0, 4, right)
+
+    def pass_to_partner():
+        wait_for(half(right, 0), ring_sem.at[9])
+        core_send(right)
+        wait_for(half(left, 1), ring_sem.at[7])
+        core_send(left)
 
     def end_weights():
-        wait_for(weights.at[far, pl.ds(0, half_rows)], ring_sem.at[6])
-        wait_for(weights.at[far, pl.ds(0, half_rows)], ring_sem.at[7])
-        remote(weights.at[far], weights.at[far], (core_sem.at[0], core_sem.at[1]), (tp, partner))
+        wait_for(half(far, 0), ring_sem.at[10])
+        wait_for(half(far, 1), ring_sem.at[11])
+        core_send(far)
         waits.append((weights.at[pl.ds(0, 4)], core_sem.at[0]))
-        wait_for(weights.at[pl.ds(0, 4)], core_sem.at[1])
-
+
+    pl.semaphore_wait(barrier, 11)
+    gather_first_wout()
+    tell(near_sem, beside(1))
     tokens_load.wait()
     first_parts()
-    pl.semaphore_wait(barrier, 21)
     send_parts()
-    gather_wout(0)
+    pl.semaphore_wait(near_sem, 4)
+    tell(line_sem, beside(2))
+    send_pair_sums()
+    pl.semaphore_wait(line_sem, 4)
+    tell(row_sem, z_peers)
     for peer in dp_peers:
         remote(gains.at[dp], gains.at[dp], (gain_sem.at[0], gain_sem.at[1]), peer)
     waits.append((gains.at[pl.ds(0, 7)], gain_sem.at[0]))
@@ -353,21 +421,24 @@
             remote(tokens.at[at_rows(peer[1]), at_column], residue, (residue_sem.at[0], residue_sem.at[1]), peer)
         residue[...] = tokens[at_rows(dp), at_column]
 
-    for peer in z_peers:
-        pl.semaphore_signal(row_sem, inc=1, device_id=peer, device_id_type=MESH)
     gather_weights()
-    pass_wout(0)
+    gather_second_wout()
+    pass_first_wout()
     projected = first_projected()
     for copy in small_loads + [state_load]:
         copy.wait()
-    mixed = mix(0, projected)
+    mixed = mix(0, projected)[:, :HEAD]
     pl.semaphore_wait(row_sem, 7)
-    for peer in dp_peers:
-        pl.semaphore_signal(plane_sem, inc=1, device_id=peer, device_id_type=MESH)
+    tell(plane_sem, dp_peers)
+    for copy in wout_loads:
+        copy.wait()
+    project_out(0, mixed, own_columns)
     wait_for(wout.at[0, pl.ds(0, 4)], wout_core_sem.at[2])
-    project_out(0, mixed)
+    project_out(0, mixed, other_columns)
     send_out(0)
     update_state(0)
+    pass_weights()
+    pass_to_partner()
 
     @pl.when(jnp.logical_not(owns_columns))
     def _():
@@ -375,19 +446,19 @@
 
     finish_share(0, residue[...])
     x_all[tp] = share[0]
-    for peer in tp_peers:
-        remote(share.at[0], x_all.at[tp], (x_sem.at[0], x_sem.at[1]), peer)
-    waits.append((x_all.at[pl.ds(0, 63)], x_sem.at[0]))
-    pass_weights()
-    gather_wout(1)
-    pass_wout(1)
+    for peer, (a, _) in zip(tp_peers, TP_OFFSETS):
+        remote(share.at[0], x_all.at[tp], (x_sem.at[8], x_sem.at[a]), peer)
+    waits.append((x_all.at[pl.ds(0, 63)], x_sem.at[8]))
+    pass_second_wout()
+    end_weights()
+    end_second_wout()
     wait_for(gains.at[pl.ds(0, 7)], gain_sem.at[1])
     pl.semaphore_wait(plane_sem, 7)
-    end_weights()
+    wait_for(weights.at[pl.ds(0, 4)], core_sem.at[1])
+
+    mixed = mix(1, second_projected())[:, :HEAD]
     wait_for(wout.at[1, pl.ds(0, 4)], wout_core_sem.at[3])
-    wait_for(x_all.at[pl.ds(0, 63)], x_sem.at[1])
-
-    project_out(1, mix(1, second_projected()))
+    project_out(1, mixed, range(8))
     send_out(1)
     update_state(1)
     finish_share(1, share[0])
@@ -471,19 +542,21 @@
             pltpu.VMEM((16, LANES), bf16),
             pltpu.VMEM((LAYERS, ROWS, 32, LANES), f32),
             pltpu.VMEM((8, ROWS, 6 * HEAD), bf16),
-            pltpu.VMEM((7, ROWS, 6 * HEAD), bf16),
+            pltpu.VMEM((4, ROWS, 6 * HEAD), bf16),
+            pltpu.VMEM((4, ROWS, 6 * HEAD), bf16),
+            pltpu.VMEM((3, ROWS, 6 * HEAD), bf16),
             pltpu.VMEM((8, 1, LANES), f32),
             pltpu.VMEM((7, 1, LANES), f32),
             pltpu.VMEM((LAYERS, 64, 16, LANES), bf16),
-            pltpu.VMEM((LAYERS, 63, 16, LANES), bf16),
+            pltpu.VMEM((LAYERS, 64, 16, LANES), bf16),
             pltpu.VMEM((LAYERS, 16, LANES), bf16),
             pltpu.VMEM((64, 16, LANES), bf16),
             pltpu.VMEM((64, 16, LANES), bf16),
         ]
         + [pltpu.VMEM((ROWS, LANES), f32)] * 6
-        + [dma((10,)), dma((9,)), dma((2,)), dma((2,)), dma((4,)), dma((2,)), dma((2,)), dma((2,))]
-        + [dma((4,)), dma((4,)), dma((8,)), dma((2,)), dma((3,))]
-        + [pltpu.SemaphoreType.REGULAR] * 2,
+        + [dma((10,)), dma((9,)), dma((2,)), dma((2,)), dma((2,)), dma((4,)), dma((9,)), dma((2,)), dma((2,))]
+        + [dma((8,)), dma((4,)), dma((12,)), dma((2,)), dma((3,))]
+        + [pltpu.SemaphoreType.REGULAR] * 4,
         compiler_params=pltpu.CompilerParams(
             collective_id=0, has_side_effects=True, vmem_limit_bytes=32 * 1024 * 1024
         ),

time: 67.9 us -> 60.8 us (0.90)
  Pallas kernels: 67.1 us -> 60 us
    pallas_call x1, Pallas kernels: 66.1 us -> 59 us  [shards(): pl.pallas_call(body, out_shape=(pltpu.VMEM((256, WIDE), bf16), pltpu.VMEM...]
where the time goes in v3:
time: 60.8 us; the launch traced here: 60.7 us
  Pallas kernels  60 us (99%)
  between operations  0.64 us (1%)
    pallas_call x1, Pallas kernels, shards(): pl.pallas_call(body, out_shape=(pltpu.VMEM((256, WIDE), bf16), pltpu.VMEM...  59 us

profile of v3, /device:TPU:1, one launch (start us, length us, event | category | flops | bytes accessed | tf_op | source)
XLA Modules:
  0.0 60.7 jit_solution(5755865804137276728)
XLA Ops:
  0.6 59.0 %blocks.1 = (bf16[256,512]{1,0:T(8,128)(2,1)S(1)}, f32[2,32,32,128]{3,2,1,0:T(8,128)S(1)}) custom-call(bf16[256,512]{1,0:T(8,128)(2,1)} %tokens_ref.1, f32[2,512]{1,0:T(2,128)} %gain_in.1, bf16[2,64,512]{2,1,0:T(8,128)(2,1)} %bitcast.9, bf16[2,64,512]{2,1,0:T(8,128)(2,1)} %bitcast.10, bf16[2,64,512]{2,1,0:T(8,128)(2,1)} %bitcast.11, ...), custom_call_target="tpu_custom_call" | custom-call | tf_op jit(solution)/shard_map/blocks/pallas_call | solution.py:526
  59.6 1.1 %write_out.1 = (bf16[256,512]{1,0:T(8,128)(2,1)}, f32[2,32,32,128]{3,2,1,0:T(8,128)}) custom-call(bf16[256,512]{1,0:T(8,128)(2,1)S(1)} %get-tuple-element.6.next_ref, f32[2,32,32,128]{3,2,1,0:T(8,128)S(1)} %get-tuple-element.7.state_ref), custom_call_target="tpu_custom_call" | custom-call | tf_op jit(solution)/shard_map/write_out/pallas_call | solution.py:578

commit v4 on v3

--- a/solution.py
+++ b/solution.py
@@ -35,6 +35,10 @@
 
 def dot(a, b):
     return jnp.dot(a, b, preferred_element_type=jnp.float32)
+
+
+def contract(a, b):
+    return lax.dot_general(a, b, (((1,), (1,)), ((), ())), preferred_element_type=jnp.float32)
 
 
 def wait_for(ref, sem):
@@ -182,9 +186,7 @@
         )
         for copy in first_loads:
             copy.wait()
-        part = lax.dot_general(
-            normed, first_weights[...], (((1,), (1,)), ((), ())), preferred_element_type=jnp.float32
-        ).astype(jnp.bfloat16)
+        part = contract(normed, first_weights[...]).astype(jnp.bfloat16)
         for o in range(8):
             part_send[o] = part[o * ROWS : (o + 1) * ROWS]
 
@@ -221,23 +223,24 @@
     def second_projected():
         squares = jnp.zeros((ROWS, LANES), jnp.float32)
         total = jnp.zeros((6 * HEAD, ROWS), jnp.float32)
-        for a in RING8 + (0,):
+        held = jnp.zeros((ROWS, 6 * HEAD), jnp.float32)
+        arrivals = ((4, 3, 5, 2), (6, 1, 7, 0))
+        for a in arrivals[0] + arrivals[1]:
             d = lax.rem(z + 8 - a, 8)
-            wait_for(x_all.at[pl.ds(0, 8 if a else 7)], x_sem.at[a])
+            for group in arrivals:
+                if a == group[0]:
+                    for other in group:
+                        wait_for(x_all.at[pl.ds(0, 8 if other else 7)], x_sem.at[other])
             pieces = []
             for c in range(4):
                 at = (d * 4 + c) * 2
                 piece = jnp.concatenate([x_all[at], x_all[at + 1]], axis=0).astype(jnp.float32)
                 squares = squares + piece * piece
                 pieces.append((piece * gains[d, 1:2, c * LANES : (c + 1) * LANES]).astype(jnp.bfloat16))
-            total = total + lax.dot_general(
-                weights[d],
-                jnp.concatenate(pieces, axis=1),
-                (((1,), (1,)), ((), ())),
-                preferred_element_type=jnp.float32,
-            )
+            total = total + contract(weights[d, :, 0 : 2 * LANES], jnp.concatenate(pieces[:2], axis=1))
+            held = held + contract(jnp.concatenate(pieces[2:], axis=1), weights[d, :, 2 * LANES :])
         inv = lax.rsqrt(jnp.sum(squares, axis=1, keepdims=True) / D + norm_floor)
-        return total.T * inv
+        return (total.T + held) * inv
 
     def mix(b, projected):
         heads = projected.astype(jnp.bfloat16).astype(jnp.float32)
@@ -355,7 +358,7 @@
         to_partner(1, far)
         waits.append((wout.at[1, pl.ds(0, 4)], wout_core_sem.at[1]))
 
-    halves = (pl.ds(0, 3 * HEAD), pl.ds(3 * HEAD, 3 * HEAD))
+    halves = (pl.ds(0, 192), pl.ds(192, 192))
 
     def half(owner, n):
         return weights.at[owner, halves[n]]
@@ -363,7 +366,7 @@
     def ring_send(owner, n, at, peer):
         there = half(owner, n)
         remote(there, there, (ring_sem.at[at], ring_sem.at[6 + at]), (tp, peer))
-        waits.append((half(0, 0), ring_sem.at[at]))
+        waits.append((half(0, n), ring_sem.at[at]))
 
     def core_send(owner):
         there = weights.at[owner]
@@ -402,11 +405,7 @@
     tokens_load.wait()
     first_parts()
     send_parts()
-    pl.semaphore_wait(near_sem, 4)
-    tell(line_sem, beside(2))
     send_pair_sums()
-    pl.semaphore_wait(line_sem, 4)
-    tell(row_sem, z_peers)
     for peer in dp_peers:
         remote(gains.at[dp], gains.at[dp], (gain_sem.at[0], gain_sem.at[1]), peer)
     waits.append((gains.at[pl.ds(0, 7)], gain_sem.at[0]))
@@ -421,6 +420,10 @@
             remote(tokens.at[at_rows(peer[1]), at_column], residue, (residue_sem.at[0], residue_sem.at[1]), peer)
         residue[...] = tokens[at_rows(dp), at_column]
 
+    pl.semaphore_wait(near_sem, 4)
+    tell(line_sem, beside(2))
+    pl.semaphore_wait(line_sem, 4)
+    tell(row_sem, z_peers)
     gather_weights()
     gather_second_wout()
     pass_first_wout()

time: 60.8 us -> 60.8 us (level)
  no operation moved by 1% of the time
where the time goes in v4:
time: 60.8 us; the launch traced here: 60.6 us
  Pallas kernels  60 us (99%)
  between operations  0.64 us (1%)
    pallas_call x1, Pallas kernels, shards(): pl.pallas_call(body, out_shape=(pltpu.VMEM((256, WIDE), bf16), pltpu.VMEM...  58.9 us

profile of v4, /device:TPU:1, one launch (start us, length us, event | category | flops | bytes accessed | tf_op | source)
XLA Modules:
  0.0 60.6 jit_solution(17033064354582656340)
XLA Ops:
  0.6 58.9 %blocks.1 = (bf16[256,512]{1,0:T(8,128)(2,1)S(1)}, f32[2,32,32,128]{3,2,1,0:T(8,128)S(1)}) custom-call(bf16[256,512]{1,0:T(8,128)(2,1)} %tokens_ref.1, f32[2,512]{1,0:T(2,128)} %gain_in.1, bf16[2,64,512]{2,1,0:T(8,128)(2,1)} %bitcast.9, bf16[2,64,512]{2,1,0:T(8,128)(2,1)} %bitcast.10, bf16[2,64,512]{2,1,0:T(8,128)(2,1)} %bitcast.11, ...), custom_call_target="tpu_custom_call" | custom-call | tf_op jit(solution)/shard_map/blocks/pallas_call | solution.py:529
  59.6 1.1 %write_out.1 = (bf16[256,512]{1,0:T(8,128)(2,1)}, f32[2,32,32,128]{3,2,1,0:T(8,128)}) custom-call(bf16[256,512]{1,0:T(8,128)(2,1)S(1)} %get-tuple-element.6.next_ref, f32[2,32,32,128]{3,2,1,0:T(8,128)S(1)} %get-tuple-element.7.state_ref), custom_call_target="tpu_custom_call" | custom-call | tf_op jit(solution)/shard_map/write_out/pallas_call | solution.py:581

commit v5 on v4

--- a/solution.py
+++ b/solution.py
@@ -136,9 +136,6 @@
         for peer in peers:
             pl.semaphore_signal(sem, inc=1, device_id=peer, device_id_type=MESH)
 
-    barrier = pltpu.get_barrier_semaphore()
-    tell(barrier, dp_peers + beside(1))
-
     def load(src, dst, sem):
         copy = pltpu.make_async_copy(src, dst, sem)
         copy.start()
@@ -157,6 +154,9 @@
         load(w.at[1], weights.at[dp, pl.ds(n * HEAD, HEAD)], late_sem.at[n + 1]) for n, w in enumerate(projections)
     ]
 
+    barrier = pltpu.get_barrier_semaphore()
+    tell(barrier, dp_peers + beside(1))
+
     lane = iota((ROWS, LANES), 1)
     row = iota((ROWS, LANES), 0)
     low_half = lane < HEAD
@@ -173,12 +173,6 @@
 
     def first_parts():
         columns = [tokens[:, c * LANES : (c + 1) * LANES].astype(jnp.float32) for c in range(4)]
-        squares = columns[0] * columns[0]
-        for c in columns[1:]:
-            squares = squares + c * c
-        totals = dot(two_terms(squares), ones)
-        for o in range(8):
-            sq_send[o] = jnp.sum(totals[o * ROWS : (o + 1) * ROWS] * eye, axis=0, keepdims=True)
         gain_load.wait()
         normed = jnp.concatenate(
             [(c * gains[dp, 0:1, n * LANES : (n + 1) * LANES]).astype(jnp.bfloat16) for n, c in enumerate(columns)],
@@ -193,9 +187,18 @@
     def send_parts():
         for chip in range(4):
             remote(part_send.at[chip * 2 + 1 - core], part_core.at[chip], (pair_sem.at[0], pair_sem.at[1]), (tp, partner))
+        waits.append((part_core, pair_sem.at[0]))
+
+    def send_squares():
+        columns = [tokens[:, c * LANES : (c + 1) * LANES].astype(jnp.float32) for c in range(4)]
+        squares = columns[0] * columns[0]
+        for c in columns[1:]:
+            squares = squares + c * c
+        totals = dot(two_terms(squares), ones)
+        for o in range(8):
+            sq_send[o] = jnp.sum(totals[o * ROWS : (o + 1) * ROWS] * eye, axis=0, keepdims=True)
         for i, peer in enumerate(dp_peers):
             remote(sq_send.at[peer[1]], sq_recv.at[i], (sq_sem.at[0], sq_sem.at[1]), peer)
-        waits.append((part_core, pair_sem.at[0]))
         waits.append((sq_recv, sq_sem.at[0]))
 
     def send_pair_sums():
@@ -405,6 +408,7 @@
     tokens_load.wait()
     first_parts()
     send_parts()
+    send_squares()
     send_pair_sums()
     for peer in dp_peers:
         remote(gains.at[dp], gains.at[dp], (gain_sem.at[0], gain_sem.at[1]), peer)

time: 60.8 us -> 61.1 us (level)
  no operation moved by 1% of the time
where the time goes in v5:
time: 61.1 us; the launch traced here: 60.9 us
  Pallas kernels  60.3 us (99%)
  between operations  0.64 us (1%)
    pallas_call x1, Pallas kernels, shards(): pl.pallas_call(body, out_shape=(pltpu.VMEM((256, WIDE), bf16), pltpu.VMEM...  59.2 us

profile of v5, /device:TPU:1, one launch (start us, length us, event | category | flops | bytes accessed | tf_op | source)
XLA Modules:
  0.0 60.9 jit_solution(3118067800297392254)
XLA Ops:
  0.6 59.2 %blocks.1 = (bf16[256,512]{1,0:T(8,128)(2,1)S(1)}, f32[2,32,32,128]{3,2,1,0:T(8,128)S(1)}) custom-call(bf16[256,512]{1,0:T(8,128)(2,1)} %tokens_ref.1, f32[2,512]{1,0:T(2,128)} %gain_in.1, bf16[2,64,512]{2,1,0:T(8,128)(2,1)} %bitcast.9, bf16[2,64,512]{2,1,0:T(8,128)(2,1)} %bitcast.10, bf16[2,64,512]{2,1,0:T(8,128)(2,1)} %bitcast.11, ...), custom_call_target="tpu_custom_call" | custom-call | tf_op jit(solution)/shard_map/blocks/pallas_call | solution.py:533
  59.9 1.1 %write_out.1 = (bf16[256,512]{1,0:T(8,128)(2,1)}, f32[2,32,32,128]{3,2,1,0:T(8,128)}) custom-call(bf16[256,512]{1,0:T(8,128)(2,1)S(1)} %get-tuple-element.6.next_ref, f32[2,32,32,128]{3,2,1,0:T(8,128)S(1)} %get-tuple-element.7.state_ref), custom_call_target="tpu_custom_call" | custom-call | tf_op jit(solution)/shard_map/write_out/pallas_call | solution.py:585
